TPU v7x, 512 devices: a whole 4x8x8 slice. The times are simulated.
512 devices in a mesh: sp: 64 (over z, y), tp: 8 (over x, core).
Axes of the slice: x: 4, y: 8, z: 8, core: 2. Of those that a mesh axis runs over, the one named last changes fastest.
Arguments:
- residual_in: bfloat16 [16384, 2048], P(('sp', 'tp')), may hold values from -6 to 6
- query_lean: bfloat16 [16384, 8, 96], P('sp', 'tp'), may hold values from -60 to 60
- query_broad: bfloat16 [16384, 8, 160], P('sp', 'tp'), may hold values from -60 to 60
- latent: bfloat16 [16384, 256], P('sp'), may hold values from -6 to 6
- rope_key: bfloat16 [16384, 32], P('sp'), may hold values from -8 to 8
- latent_gain: float32 [256], replicated, may hold values from 0.1 to 1.9
- key_up_lean: bfloat16 [256, 8, 64], P(None, 'tp'), may hold values from -0.375 to 0.375
- key_up_broad: bfloat16 [256, 8, 128], P(None, 'tp'), may hold values from -0.375 to 0.375
- value_up_lean: bfloat16 [256, 8, 64], P(None, 'tp'), may hold values from -0.375 to 0.375
- value_up_broad: bfloat16 [256, 8, 128], P(None, 'tp'), may hold values from -0.375 to 0.375
- out_lean: bfloat16 [8, 64, 2048], P('tp'), may hold values from -0.15625 to 0.15625
- out_broad: bfloat16 [8, 128, 2048], P('tp'), may hold values from -0.15625 to 0.15625
- attn_gain: float32 [2048], replicated, may hold values from 0.1 to 1.9
- mlp_gain: float32 [2048], replicated, may hold values from 0.1 to 1.9
- gate_weight: bfloat16 [2048, 2816], P('sp', 'tp'), may hold values from -0.125 to 0.125
- up_weight: bfloat16 [2048, 2816], P('sp', 'tp'), may hold values from -0.125 to 0.125
- down_weight: bfloat16 [2816, 2048], P('tp', 'sp'), may hold values from -0.109375 to 0.109375
Outputs:
- layer_out: bfloat16 [16384, 2048], P(('sp', 'tp'))
All inputs are finite; a program needn't handle non-finite values.
Results may differ from a plain program's by a relative error of at most 0.015.
Values may be sent and summed in bfloat16 or wider, within the bound.
A program may use at most 128 MiB of HBM per device.

v0:
```python
import math

import jax
import jax.numpy as jnp
from jax import lax
from jax.sharding import PartitionSpec as P

THETA = 10000.0
EPS = 1e-06
NEGATIVE = -1e30


def in_one_piece(arrays, axis, dim, along):
    both = jnp.concatenate(arrays, axis=along)
    out, at, finished = (lax.all_gather(both, axis, axis=dim, tiled=True), 0, [])
    for a in arrays:
        finished.append(lax.slice_in_dim(out, at, at + a.shape[along], axis=along))
        at += a.shape[along]
    return tuple(finished)


def cut_along(x, dim, devices):
    before, after = (x.shape[:dim], x.shape[dim + 1 :])
    return jnp.moveaxis(x.reshape(*before, devices, -1, *after), dim, 0)


def sent_and_summed(x, axis, dim):
    devices = lax.axis_size(axis)
    tiles = lax.all_to_all(cut_along(x, dim, devices), axis, 0, 0, tiled=True)
    return jnp.sum(tiles.astype(jnp.float32), axis=0)


def in_order(tiles, dim):
    tiles = jnp.moveaxis(tiles, 0, dim)
    lengths = tiles.shape
    return tiles.reshape(*lengths[:dim], lengths[dim] * lengths[dim + 1], *lengths[dim + 2 :])


def sent_to_all(x, axis):
    devices = lax.axis_size(axis)
    return lax.all_to_all(jnp.broadcast_to(x[None], (devices, *x.shape)), axis, 0, 0, tiled=True)


def gathered_copies(x, axis, dim):
    return in_order(sent_to_all(x, axis), dim)


def gather_turned(arrays, axis, dims):
    turned = [jnp.moveaxis(a, dim, 0) for a, dim in zip(arrays, dims)]
    both = jnp.concatenate([t.reshape(len(t), -1) for t in turned], axis=1)
    out, at, finished = (lax.all_gather(both, axis, axis=0, tiled=True), 0, [])
    for t, dim in zip(turned, dims):
        section = out[:, at : at + t[0].size].reshape(-1, *t.shape[1:])
        finished.append(jnp.moveaxis(section, 0, dim))
        at += t[0].size
    return tuple(finished)


def rotate(values, positions):
    width = values.shape[-1]
    half = width // 2
    freqs = THETA ** (-2.0 * jnp.arange(half, dtype=jnp.float32) / width)
    angle = positions.astype(jnp.float32)[:, None] * freqs[None, :]
    cosine = jnp.cos(angle)
    sine = jnp.sin(angle)
    if values.ndim == 3:
        cosine = cosine[:, None, :]
        sine = sine[:, None, :]
    first = values[..., :half]
    second = values[..., half:]
    return jnp.concatenate(
        [first * cosine - second * sine, first * sine + second * cosine], axis=-1
    )


def normalize(values, gain):
    return values * lax.rsqrt(jnp.mean(values * values, axis=-1, keepdims=True) + EPS) * gain


def block_keys(weights, latent_rows):
    projected = []
    for key_up, value_up in weights:
        keys = jnp.einsum(
            "kr,rhd->khd", latent_rows, key_up, preferred_element_type=jnp.float32
        ).astype(jnp.bfloat16)
        values = jnp.einsum(
            "kr,rhd->khd", latent_rows, value_up, preferred_element_type=jnp.float32
        ).astype(jnp.bfloat16)
        projected.append((keys, values))
    return projected


def attend(carry, queries, projected, rotated_rows, key_pos, query_pos):
    updated = []
    visible = key_pos[None, :] <= query_pos[:, None]
    for state, query, pair in zip(carry, queries, projected):
        query_nope, query_rot, scale = query
        keys, values = pair
        peak, total, accum = state
        scores = (
            jnp.einsum("qhd,khd->hqk", query_nope, keys, preferred_element_type=jnp.float32)
            + jnp.einsum("qhr,kr->hqk", query_rot, rotated_rows, preferred_element_type=jnp.float32)
        ) * scale
        scores = jnp.where(visible[None], scores, NEGATIVE)
        new_peak = jnp.maximum(peak, jnp.max(scores, axis=-1))
        weights = jnp.where(visible[None], jnp.exp(scores - new_peak[..., None]), 0.0)
        factor = jnp.exp(peak - new_peak)
        total = total * factor + jnp.sum(weights, axis=-1)
        accum = accum * factor[..., None] + jnp.einsum(
            "hqk,khv->hqv", weights.astype(jnp.bfloat16), values, preferred_element_type=jnp.float32
        )
        updated.append((new_peak, total, accum))
    return tuple(updated)


def fold_piece(carry, latent_piece, rotated_piece, piece_pos, weights, segments):
    count = latent_piece.shape[0]
    block = math.gcd(count, 1024)
    last_all = segments[0][1][-1]

    def one_block(index, state):
        lat_rows = lax.dynamic_slice_in_dim(latent_piece, index * block, block, 0)
        rot_rows = lax.dynamic_slice_in_dim(rotated_piece, index * block, block, 0)
        pos_rows = lax.dynamic_slice_in_dim(piece_pos, index * block, block, 0)
        first_key = jnp.min(pos_rows)

        def work(inner):
            projected = block_keys(weights, lat_rows)
            results = []
            for inner_seg, segment in zip(inner, segments):
                queries, seg_pos = segment
                results.append(
                    lax.cond(
                        first_key <= seg_pos[-1],
                        lambda held, queries=queries, seg_pos=seg_pos: attend(
                            held, queries, projected, rot_rows, pos_rows, seg_pos
                        ),
                        lambda held: held,
                        inner_seg,
                    )
                )
            return tuple(results)

        return lax.cond(first_key <= last_all, work, lambda inner: inner, state)

    return lax.fori_loop(0, count // block, one_block, carry)


def shards(
    residual_in,
    query_lean,
    query_broad,
    latent,
    rope_key,
    latent_gain,
    key_up_lean,
    key_up_broad,
    value_up_lean,
    value_up_broad,
    out_lean,
    out_broad,
    attn_gain,
    mlp_gain,
    gate_weight,
    up_weight,
    down_weight,
):
    tokens_here = query_lean.shape[0]
    n_tp = lax.axis_size("tp")
    share = tokens_here // n_tp
    sp_index = lax.axis_index("sp")
    first = sp_index * tokens_here
    query_pos = first + jnp.arange(tokens_here, dtype=jnp.int32)
    rope_width = rope_key.shape[1]
    weights = ((key_up_lean, value_up_lean), (key_up_broad, value_up_broad))
    segment_rows = (query_lean, query_broad, query_pos)
    segments = []
    initial = []
    lean_rows, broad_rows, seg_pos = segment_rows
    queries = []
    states = []
    for query, value_up in ((lean_rows, value_up_lean), (broad_rows, value_up_broad)):
        nope = query.shape[2] - rope_width
        query_rot = rotate(query[:, :, nope:].astype(jnp.float32), seg_pos).astype(jnp.bfloat16)
        queries.append((query[:, :, :nope], query_rot, query.shape[2] ** (-0.5)))
        heads = query.shape[1]
        rows = query.shape[0]
        states.append(
            (
                jnp.full((heads, rows), NEGATIVE, jnp.float32),
                jnp.zeros((heads, rows), jnp.float32),
                jnp.zeros((heads, rows, value_up.shape[2]), jnp.float32),
            )
        )
    segments.append((tuple(queries), seg_pos))
    initial.append(tuple(states))
    segments = tuple(segments)
    initial = tuple(initial)
    sent_latent = normalize(latent.astype(jnp.float32), latent_gain).astype(jnp.bfloat16)
    sent_rot = rotate(rope_key.astype(jnp.float32), query_pos).astype(jnp.bfloat16)
    pieces = in_one_piece((sent_latent, sent_rot), "sp", 0, 1)
    piece_pos = jnp.arange(pieces[0].shape[0], dtype=jnp.int32)
    folded = fold_piece(initial, pieces[0], pieces[1], piece_pos, weights, segments)
    results = [
        [(accum / total[..., None]).astype(jnp.bfloat16) for peak, total, accum in seg_state]
        for seg_state in folded
    ]
    attended = results[0]
    term = jnp.zeros((share * lax.axis_size("tp"), out_lean.shape[2]), jnp.float32)
    for rows_all, weight in ((attended[0], out_lean), (attended[1], out_broad)):
        rows = rows_all
        term = term + jnp.einsum("hqv,hvd->qd", rows, weight, preferred_element_type=jnp.float32)
    head_sum = sent_and_summed(term.astype(jnp.bfloat16), "tp", 0)
    branch = normalize(head_sum, attn_gain)
    kept = (residual_in.astype(jnp.float32) + branch).astype(jnp.bfloat16)
    normed = normalize(kept.astype(jnp.float32), mlp_gain).astype(jnp.bfloat16)
    whole_normed = gathered_copies(normed, "tp", 0)
    gate_whole, up_whole, down_whole = gather_turned(
        (gate_weight, up_weight, down_weight), "sp", (0, 0, 1)
    )
    gate = jnp.dot(whole_normed, gate_whole, preferred_element_type=jnp.float32)
    up = jnp.dot(whole_normed, up_whole, preferred_element_type=jnp.float32)
    hidden = (jax.nn.silu(gate) * up).astype(jnp.bfloat16)
    rows = hidden
    channel_sum = sent_and_summed(
        jnp.dot(rows, down_whole, preferred_element_type=jnp.float32).astype(jnp.bfloat16), "tp", 0
    )
    return (kept.astype(jnp.float32) + 0.5 * channel_sum).astype(jnp.bfloat16)


def solution(mesh):
    in_specs = (
        P(("sp", "tp"), None),
        P("sp", "tp", None),
        P("sp", "tp", None),
        P("sp", None),
        P("sp", None),
        P(),
        P(None, "tp", None),
        P(None, "tp", None),
        P(None, "tp", None),
        P(None, "tp", None),
        P("tp", None, None),
        P("tp", None, None),
        P(),
        P(),
        P("sp", "tp"),
        P("sp", "tp"),
        P("tp", "sp"),
    )
    out_specs = P(("sp", "tp"), None)
    return jax.shard_map(shards, mesh=mesh, in_specs=in_specs, out_specs=out_specs, check_vma=False)
```

profile of v0, /device:TPU:480, one launch (start us, length us, event | category | flops | bytes accessed | tf_op | source)
XLA Modules:
  0.0 437.6 jit_solution(8570360309762262928)
XLA Ops:
  15.5 111.2 %all-gather.3.cloned.1.call-done = bf16[16384,288]{1,0:T(8,128)(2,1)} async-done(((bf16[256,288]{1,0:T(8,128)(2,1)}), bf16[16384,288]{1,0:T(8,128)(2,1)}) %all-gather.3.cloned.1.call-update) | async-done | bytes 9437200 | tf_op jit(solution)/shard_map/all_gather | solution.py:15
  126.6 7.0 %slice.71 = bf16[16384,256]{1,0:T(8,128)(2,1)} slice(bf16[16384,288]{1,0:T(8,128)(2,1)} %all-gather.3.cloned.1.call-done), slice={[0:16384], [0:256]} | slice | bytes 16777216 | tf_op jit(solution)/shard_map/slice | solution.py:17
  137.6 224.7 %while.24 = (s32[]{:T(128)}, f32[1,256]{1,0:T(1,128)S(1)}, f32[1,256]{1,0:T(1,128)S(1)}, f32[1,256,64]{1,2,0:T(8,128)S(1)}, f32[1,256]{1,0:T(1,128)S(1)}, /*inde...) while((s32[]{:T(128)}, f32[1,256]{1,0:T(1,128)S(1)}, ...), condition=%wide.region_11.12_spmd.clone, body=%wide.region_1.11_spmd.clone.sunk | while | flops 443255040 | bytes 15474435 | solution.py:146
  139.5 12.1 %conditional.4 = ((f32[1,256]{1,0:T(1,128)S(1)}, f32[1,256]{1,0:T(1,128)S(1)}, f32[1,256,64]{1,2,0:T(8,128)S(1)}, f32[1,256]{1,0:T(1,128)S(1)}, f32[1,256]{1,0:T(1,128)S(1)}, /*index=5*/f32[1,256,128]{2,1,0:T(8,128)S(1)})) conditional(s32[]{:T(128)} %convert_element_type.200, (f32[1,256]{1,0:T(1,128)S(1)}, f32[1,256]{1,0:T(1,128)S(1)}, ...), branch_computations={%region_3.0_spmd, %region_4.10_spmd} | conditional | flops 443254016 | bytes 15464722 | solution.py:144
  153.5 12.1 %conditional.4 = ((f32[1,256]{1,0:T(1,128)S(1)}, f32[1,256]{1,0:T(1,128)S(1)}, f32[1,256,64]{1,2,0:T(8,128)S(1)}, f32[1,256]{1,0:T(1,128)S(1)}, f32[1,256]{1,0:T(1,128)S(1)}, /*index=5*/f32[1,256,128]{2,1,0:T(8,128)S(1)})) conditional(s32[]{:T(128)} %convert_element_type.200, (f32[1,256]{1,0:T(1,128)S(1)}, f32[1,256]{1,0:T(1,128)S(1)}, ...), branch_computations={%region_3.0_spmd, %region_4.10_spmd} | conditional | flops 443254016 | bytes 15464722 | solution.py:144
  167.6 12.1 %conditional.4 = ((f32[1,256]{1,0:T(1,128)S(1)}, f32[1,256]{1,0:T(1,128)S(1)}, f32[1,256,64]{1,2,0:T(8,128)S(1)}, f32[1,256]{1,0:T(1,128)S(1)}, f32[1,256]{1,0:T(1,128)S(1)}, /*index=5*/f32[1,256,128]{2,1,0:T(8,128)S(1)})) conditional(s32[]{:T(128)} %convert_element_type.200, (f32[1,256]{1,0:T(1,128)S(1)}, f32[1,256]{1,0:T(1,128)S(1)}, ...), branch_computations={%region_3.0_spmd, %region_4.10_spmd} | conditional | flops 443254016 | bytes 15464722 | solution.py:144
  174.7 5.0 %conditional = ((f32[1,256]{1,0:T(1,128)S(1)}, f32[1,256]{1,0:T(1,128)S(1)}, f32[1,256,64]{1,2,0:T(8,128)S(1)}, f32[1,256]{1,0:T(1,128)S(1)}, f32[1,256]{1,0:T(1,128)S(1)}, /*index=5*/f32[1,256,128]{2,1,0:T(8,128)S(1)})) conditional(s32[]{:T(128)} %convert_element_type.100, (f32[1,256]{1,0:T(1,128)S(1)}, f32[1,256]{1,0:T(1,128)S(1)}, ...), branch_computations={%region_5.0_spmd, %region_6.9_spmd} | conditional | flops 241533952 | bytes 12380216 | solution.py:133
  181.6 12.2 %conditional.4 = ((f32[1,256]{1,0:T(1,128)S(1)}, f32[1,256]{1,0:T(1,128)S(1)}, f32[1,256,64]{1,2,0:T(8,128)S(1)}, f32[1,256]{1,0:T(1,128)S(1)}, f32[1,256]{1,0:T(1,128)S(1)}, /*index=5*/f32[1,256,128]{2,1,0:T(8,128)S(1)})) conditional(s32[]{:T(128)} %convert_element_type.200, (f32[1,256]{1,0:T(1,128)S(1)}, f32[1,256]{1,0:T(1,128)S(1)}, ...), branch_computations={%region_3.0_spmd, %region_4.10_spmd} | conditional | flops 443254016 | bytes 15464722 | solution.py:144
  188.9 5.0 %conditional = ((f32[1,256]{1,0:T(1,128)S(1)}, f32[1,256]{1,0:T(1,128)S(1)}, f32[1,256,64]{1,2,0:T(8,128)S(1)}, f32[1,256]{1,0:T(1,128)S(1)}, f32[1,256]{1,0:T(1,128)S(1)}, /*index=5*/f32[1,256,128]{2,1,0:T(8,128)S(1)})) conditional(s32[]{:T(128)} %convert_element_type.100, (f32[1,256]{1,0:T(1,128)S(1)}, f32[1,256]{1,0:T(1,128)S(1)}, ...), branch_computations={%region_5.0_spmd, %region_6.9_spmd} | conditional | flops 241533952 | bytes 12380216 | solution.py:133
  195.8 12.1 %conditional.4 = ((f32[1,256]{1,0:T(1,128)S(1)}, f32[1,256]{1,0:T(1,128)S(1)}, f32[1,256,64]{1,2,0:T(8,128)S(1)}, f32[1,256]{1,0:T(1,128)S(1)}, f32[1,256]{1,0:T(1,128)S(1)}, /*index=5*/f32[1,256,128]{2,1,0:T(8,128)S(1)})) conditional(s32[]{:T(128)} %convert_element_type.200, (f32[1,256]{1,0:T(1,128)S(1)}, f32[1,256]{1,0:T(1,128)S(1)}, ...), branch_computations={%region_3.0_spmd, %region_4.10_spmd} | conditional | flops 443254016 | bytes 15464722 | solution.py:144
  202.9 5.0 %conditional = ((f32[1,256]{1,0:T(1,128)S(1)}, f32[1,256]{1,0:T(1,128)S(1)}, f32[1,256,64]{1,2,0:T(8,128)S(1)}, f32[1,256]{1,0:T(1,128)S(1)}, f32[1,256]{1,0:T(1,128)S(1)}, /*index=5*/f32[1,256,128]{2,1,0:T(8,128)S(1)})) conditional(s32[]{:T(128)} %convert_element_type.100, (f32[1,256]{1,0:T(1,128)S(1)}, f32[1,256]{1,0:T(1,128)S(1)}, ...), branch_computations={%region_5.0_spmd, %region_6.9_spmd} | conditional | flops 241533952 | bytes 12380216 | solution.py:133
  209.9 12.1 %conditional.4 = ((f32[1,256]{1,0:T(1,128)S(1)}, f32[1,256]{1,0:T(1,128)S(1)}, f32[1,256,64]{1,2,0:T(8,128)S(1)}, f32[1,256]{1,0:T(1,128)S(1)}, f32[1,256]{1,0:T(1,128)S(1)}, /*index=5*/f32[1,256,128]{2,1,0:T(8,128)S(1)})) conditional(s32[]{:T(128)} %convert_element_type.200, (f32[1,256]{1,0:T(1,128)S(1)}, f32[1,256]{1,0:T(1,128)S(1)}, ...), branch_computations={%region_3.0_spmd, %region_4.10_spmd} | conditional | flops 443254016 | bytes 15464722 | solution.py:144
  217.0 5.0 %conditional = ((f32[1,256]{1,0:T(1,128)S(1)}, f32[1,256]{1,0:T(1,128)S(1)}, f32[1,256,64]{1,2,0:T(8,128)S(1)}, f32[1,256]{1,0:T(1,128)S(1)}, f32[1,256]{1,0:T(1,128)S(1)}, /*index=5*/f32[1,256,128]{2,1,0:T(8,128)S(1)})) conditional(s32[]{:T(128)} %convert_element_type.100, (f32[1,256]{1,0:T(1,128)S(1)}, f32[1,256]{1,0:T(1,128)S(1)}, ...), branch_computations={%region_5.0_spmd, %region_6.9_spmd} | conditional | flops 241533952 | bytes 12380216 | solution.py:133
  223.9 12.1 %conditional.4 = ((f32[1,256]{1,0:T(1,128)S(1)}, f32[1,256]{1,0:T(1,128)S(1)}, f32[1,256,64]{1,2,0:T(8,128)S(1)}, f32[1,256]{1,0:T(1,128)S(1)}, f32[1,256]{1,0:T(1,128)S(1)}, /*index=5*/f32[1,256,128]{2,1,0:T(8,128)S(1)})) conditional(s32[]{:T(128)} %convert_element_type.200, (f32[1,256]{1,0:T(1,128)S(1)}, f32[1,256]{1,0:T(1,128)S(1)}, ...), branch_computations={%region_3.0_spmd, %region_4.10_spmd} | conditional | flops 443254016 | bytes 15464722 | solution.py:144
  237.9 12.1 %conditional.4 = ((f32[1,256]{1,0:T(1,128)S(1)}, f32[1,256]{1,0:T(1,128)S(1)}, f32[1,256,64]{1,2,0:T(8,128)S(1)}, f32[1,256]{1,0:T(1,128)S(1)}, f32[1,256]{1,0:T(1,128)S(1)}, /*index=5*/f32[1,256,128]{2,1,0:T(8,128)S(1)})) conditional(s32[]{:T(128)} %convert_element_type.200, (f32[1,256]{1,0:T(1,128)S(1)}, f32[1,256]{1,0:T(1,128)S(1)}, ...), branch_computations={%region_3.0_spmd, %region_4.10_spmd} | conditional | flops 443254016 | bytes 15464722 | solution.py:144
  245.1 5.0 %conditional = ((f32[1,256]{1,0:T(1,128)S(1)}, f32[1,256]{1,0:T(1,128)S(1)}, f32[1,256,64]{1,2,0:T(8,128)S(1)}, f32[1,256]{1,0:T(1,128)S(1)}, f32[1,256]{1,0:T(1,128)S(1)}, /*index=5*/f32[1,256,128]{2,1,0:T(8,128)S(1)})) conditional(s32[]{:T(128)} %convert_element_type.100, (f32[1,256]{1,0:T(1,128)S(1)}, f32[1,256]{1,0:T(1,128)S(1)}, ...), branch_computations={%region_5.0_spmd, %region_6.9_spmd} | conditional | flops 241533952 | bytes 12380216 | solution.py:133
  251.9 12.1 %conditional.4 = ((f32[1,256]{1,0:T(1,128)S(1)}, f32[1,256]{1,0:T(1,128)S(1)}, f32[1,256,64]{1,2,0:T(8,128)S(1)}, f32[1,256]{1,0:T(1,128)S(1)}, f32[1,256]{1,0:T(1,128)S(1)}, /*index=5*/f32[1,256,128]{2,1,0:T(8,128)S(1)})) conditional(s32[]{:T(128)} %convert_element_type.200, (f32[1,256]{1,0:T(1,128)S(1)}, f32[1,256]{1,0:T(1,128)S(1)}, ...), branch_computations={%region_3.0_spmd, %region_4.10_spmd} | conditional | flops 443254016 | bytes 15464722 | solution.py:144
  259.1 5.0 %conditional = ((f32[1,256]{1,0:T(1,128)S(1)}, f32[1,256]{1,0:T(1,128)S(1)}, f32[1,256,64]{1,2,0:T(8,128)S(1)}, f32[1,256]{1,0:T(1,128)S(1)}, f32[1,256]{1,0:T(1,128)S(1)}, /*index=5*/f32[1,256,128]{2,1,0:T(8,128)S(1)})) conditional(s32[]{:T(128)} %convert_element_type.100, (f32[1,256]{1,0:T(1,128)S(1)}, f32[1,256]{1,0:T(1,128)S(1)}, ...), branch_computations={%region_5.0_spmd, %region_6.9_spmd} | conditional | flops 241533952 | bytes 12380216 | solution.py:133
  266.0 12.1 %conditional.4 = ((f32[1,256]{1,0:T(1,128)S(1)}, f32[1,256]{1,0:T(1,128)S(1)}, f32[1,256,64]{1,2,0:T(8,128)S(1)}, f32[1,256]{1,0:T(1,128)S(1)}, f32[1,256]{1,0:T(1,128)S(1)}, /*index=5*/f32[1,256,128]{2,1,0:T(8,128)S(1)})) conditional(s32[]{:T(128)} %convert_element_type.200, (f32[1,256]{1,0:T(1,128)S(1)}, f32[1,256]{1,0:T(1,128)S(1)}, ...), branch_computations={%region_3.0_spmd, %region_4.10_spmd} | conditional | flops 443254016 | bytes 15464722 | solution.py:144
  273.1 5.0 %conditional = ((f32[1,256]{1,0:T(1,128)S(1)}, f32[1,256]{1,0:T(1,128)S(1)}, f32[1,256,64]{1,2,0:T(8,128)S(1)}, f32[1,256]{1,0:T(1,128)S(1)}, f32[1,256]{1,0:T(1,128)S(1)}, /*index=5*/f32[1,256,128]{2,1,0:T(8,128)S(1)})) conditional(s32[]{:T(128)} %convert_element_type.100, (f32[1,256]{1,0:T(1,128)S(1)}, f32[1,256]{1,0:T(1,128)S(1)}, ...), branch_computations={%region_5.0_spmd, %region_6.9_spmd} | conditional | flops 241533952 | bytes 12380216 | solution.py:133
  280.0 12.1 %conditional.4 = ((f32[1,256]{1,0:T(1,128)S(1)}, f32[1,256]{1,0:T(1,128)S(1)}, f32[1,256,64]{1,2,0:T(8,128)S(1)}, f32[1,256]{1,0:T(1,128)S(1)}, f32[1,256]{1,0:T(1,128)S(1)}, /*index=5*/f32[1,256,128]{2,1,0:T(8,128)S(1)})) conditional(s32[]{:T(128)} %convert_element_type.200, (f32[1,256]{1,0:T(1,128)S(1)}, f32[1,256]{1,0:T(1,128)S(1)}, ...), branch_computations={%region_3.0_spmd, %region_4.10_spmd} | conditional | flops 443254016 | bytes 15464722 | solution.py:144
  287.2 5.0 %conditional = ((f32[1,256]{1,0:T(1,128)S(1)}, f32[1,256]{1,0:T(1,128)S(1)}, f32[1,256,64]{1,2,0:T(8,128)S(1)}, f32[1,256]{1,0:T(1,128)S(1)}, f32[1,256]{1,0:T(1,128)S(1)}, /*index=5*/f32[1,256,128]{2,1,0:T(8,128)S(1)})) conditional(s32[]{:T(128)} %convert_element_type.100, (f32[1,256]{1,0:T(1,128)S(1)}, f32[1,256]{1,0:T(1,128)S(1)}, ...), branch_computations={%region_5.0_spmd, %region_6.9_spmd} | conditional | flops 241533952 | bytes 12380216 | solution.py:133
  294.1 12.1 %conditional.4 = ((f32[1,256]{1,0:T(1,128)S(1)}, f32[1,256]{1,0:T(1,128)S(1)}, f32[1,256,64]{1,2,0:T(8,128)S(1)}, f32[1,256]{1,0:T(1,128)S(1)}, f32[1,256]{1,0:T(1,128)S(1)}, /*index=5*/f32[1,256,128]{2,1,0:T(8,128)S(1)})) conditional(s32[]{:T(128)} %convert_element_type.200, (f32[1,256]{1,0:T(1,128)S(1)}, f32[1,256]{1,0:T(1,128)S(1)}, ...), branch_computations={%region_3.0_spmd, %region_4.10_spmd} | conditional | flops 443254016 | bytes 15464722 | solution.py:144
  301.2 5.0 %conditional = ((f32[1,256]{1,0:T(1,128)S(1)}, f32[1,256]{1,0:T(1,128)S(1)}, f32[1,256,64]{1,2,0:T(8,128)S(1)}, f32[1,256]{1,0:T(1,128)S(1)}, f32[1,256]{1,0:T(1,128)S(1)}, /*index=5*/f32[1,256,128]{2,1,0:T(8,128)S(1)})) conditional(s32[]{:T(128)} %convert_element_type.100, (f32[1,256]{1,0:T(1,128)S(1)}, f32[1,256]{1,0:T(1,128)S(1)}, ...), branch_computations={%region_5.0_spmd, %region_6.9_spmd} | conditional | flops 241533952 | bytes 12380216 | solution.py:133
  308.1 12.1 %conditional.4 = ((f32[1,256]{1,0:T(1,128)S(1)}, f32[1,256]{1,0:T(1,128)S(1)}, f32[1,256,64]{1,2,0:T(8,128)S(1)}, f32[1,256]{1,0:T(1,128)S(1)}, f32[1,256]{1,0:T(1,128)S(1)}, /*index=5*/f32[1,256,128]{2,1,0:T(8,128)S(1)})) conditional(s32[]{:T(128)} %convert_element_type.200, (f32[1,256]{1,0:T(1,128)S(1)}, f32[1,256]{1,0:T(1,128)S(1)}, ...), branch_computations={%region_3.0_spmd, %region_4.10_spmd} | conditional | flops 443254016 | bytes 15464722 | solution.py:144
  322.1 12.1 %conditional.4 = ((f32[1,256]{1,0:T(1,128)S(1)}, f32[1,256]{1,0:T(1,128)S(1)}, f32[1,256,64]{1,2,0:T(8,128)S(1)}, f32[1,256]{1,0:T(1,128)S(1)}, f32[1,256]{1,0:T(1,128)S(1)}, /*index=5*/f32[1,256,128]{2,1,0:T(8,128)S(1)})) conditional(s32[]{:T(128)} %convert_element_type.200, (f32[1,256]{1,0:T(1,128)S(1)}, f32[1,256]{1,0:T(1,128)S(1)}, ...), branch_computations={%region_3.0_spmd, %region_4.10_spmd} | conditional | flops 443254016 | bytes 15464722 | solution.py:144
  336.2 12.1 %conditional.4 = ((f32[1,256]{1,0:T(1,128)S(1)}, f32[1,256]{1,0:T(1,128)S(1)}, f32[1,256,64]{1,2,0:T(8,128)S(1)}, f32[1,256]{1,0:T(1,128)S(1)}, f32[1,256]{1,0:T(1,128)S(1)}, /*index=5*/f32[1,256,128]{2,1,0:T(8,128)S(1)})) conditional(s32[]{:T(128)} %convert_element_type.200, (f32[1,256]{1,0:T(1,128)S(1)}, f32[1,256]{1,0:T(1,128)S(1)}, ...), branch_computations={%region_3.0_spmd, %region_4.10_spmd} | conditional | flops 443254016 | bytes 15464722 | solution.py:144
  350.2 12.1 %conditional.4 = ((f32[1,256]{1,0:T(1,128)S(1)}, f32[1,256]{1,0:T(1,128)S(1)}, f32[1,256,64]{1,2,0:T(8,128)S(1)}, f32[1,256]{1,0:T(1,128)S(1)}, f32[1,256]{1,0:T(1,128)S(1)}, /*index=5*/f32[1,256,128]{2,1,0:T(8,128)S(1)})) conditional(s32[]{:T(128)} %convert_element_type.200, (f32[1,256]{1,0:T(1,128)S(1)}, f32[1,256]{1,0:T(1,128)S(1)}, ...), branch_computations={%region_3.0_spmd, %region_4.10_spmd} | conditional | flops 443254016 | bytes 15464722 | solution.py:144
  357.4 5.0 %conditional = ((f32[1,256]{1,0:T(1,128)S(1)}, f32[1,256]{1,0:T(1,128)S(1)}, f32[1,256,64]{1,2,0:T(8,128)S(1)}, f32[1,256]{1,0:T(1,128)S(1)}, f32[1,256]{1,0:T(1,128)S(1)}, /*index=5*/f32[1,256,128]{2,1,0:T(8,128)S(1)})) conditional(s32[]{:T(128)} %convert_element_type.100, (f32[1,256]{1,0:T(1,128)S(1)}, f32[1,256]{1,0:T(1,128)S(1)}, ...), branch_computations={%region_5.0_spmd, %region_6.9_spmd} | conditional | flops 241533952 | bytes 12380216 | solution.py:133
  363.3 20.0 %all_to_all.15 = bf16[8,32,2048]{2,1,0:T(8,128)(2,1)S(1)} all-to-all(bf16[8,32,2048]{2,1,0:T(8,128)(2,1)S(1)} %bitcast.100), channel_id=1, replica_groups=mesh['sp'=64,'tp'=8] {'tp'}, dimensions={0} | all-to-all | bytes 2097152 | tf_op jit(solution)/shard_map/all_to_all | solution.py:29
  388.7 15.8 %all-to-all-done.1 = bf16[8,32,2048]{2,1,0:T(8,128)(2,1)S(1)} async-done(((bf16[8,32,2048]{2,1,0:T(8,128)(2,1)}), bf16[8,32,2048]{2,1,0:T(8,128)(2,1)S(1)}, u32[]{:S(2)}, u32[]{:S(2)}) %all-to-all-start.1) | async-done | bytes 1048608 | tf_op jit(solution)/shard_map/all_to_all | solution.py:41
  411.5 18.4 %all_to_all.16 = bf16[8,32,2048]{2,1,0:T(8,128)(2,1)S(1)} all-to-all(bf16[8,32,2048]{2,1,0:T(8,128)(2,1)S(1)} %bitcast.103), channel_id=1, replica_groups=mesh['sp'=64,'tp'=8] {'tp'}, dimensions={0} | all-to-all | bytes 2097152 | tf_op jit(solution)/shard_map/all_to_all | solution.py:29
  (390 shorter events, 240.3 us)
Async XLA Ops:
  6.5 355.8 %copy-start = (bf16[1,128,2048]{2,1,0:T(8,128)(2,1)S(1)}, bf16[1,128,2048]{2,1,0:T(8,128)(2,1)}, u32[]{:S(2)}) copy-start(bf16[1,128,2048]{2,1,0:T(8,128)(2,1)} %param.34) | copy-start | bytes 1572868
  6.5 120.1 %all-gather.3.cloned.1.call-start = ((), (), s32[]{:S(2)}) async-start(), calls=%async_computation.3 | async-start | bytes 12779520 | tf_op jit(solution)/shard_map/all_gather | solution.py:15
  10.6 378.1 %all-gather.5.cloned.1.call-start = ((), (), s32[]{:S(2)}) async-start(), calls=%async_computation.4 | async-start | bytes 4792320 | tf_op jit(solution)/shard_map/all_gather | solution.py:51
  133.7 3.9 copy-start.1
  133.7 3.9 copy-start.2
  133.7 3.9 copy-start.3
  133.7 3.9 copy-start.4
  137.6 225.3 %copy-start.5 = (bf16[1,64,2048]{2,1,0:T(8,128)(2,1)S(1)}, bf16[1,64,2048]{2,1,0:T(8,128)(2,1)}, u32[]{:S(2)}) copy-start(bf16[1,64,2048]{2,1,0:T(8,128)(2,1)} %param.33) | copy-start | bytes 786436
  362.8 20.8 %copy-start.6 = (bf16[32,2048]{1,0:T(8,128)(2,1)S(1)}, bf16[32,2048]{1,0:T(8,128)(2,1)}, u32[]{:S(2)}) copy-start(bf16[32,2048]{1,0:T(8,128)(2,1)} %param.23) | copy-start | bytes 393220
  362.8 20.8 %copy-start.7 = (f32[2048]{0:T(1024)S(1)}, f32[2048]{0:T(1024)}, u32[]{:S(2)}) copy-start(f32[2048]{0:T(1024)} %param.35) | copy-start | bytes 24580
  362.8 21.1 %copy-start.8 = (f32[2048]{0:T(1024)S(1)}, f32[2048]{0:T(1024)}, u32[]{:S(2)}) copy-start(f32[2048]{0:T(1024)} %param.36) | copy-start | bytes 24580
  385.1 19.4 %all-to-all-start.1 = ((bf16[8,32,2048]{2,1,0:T(8,128)(2,1)}), bf16[8,32,2048]{2,1,0:T(8,128)(2,1)S(1)}, u32[]{:S(2)}, u32[]{:S(2)}) async-start(bf16[8,32,2048]{2,1,0:T(8,128)(2,1)} %broadcast_in_dim.19), calls=%async_computation.1 | async-start | bytes 2097152 | tf_op jit(solution)/shard_map/all_to_all | solution.py:41
Sparse Core Ops, SparseCore 0:
  10.7 115.8 all-gather.2
  129.6 84.4 all-gather.4
where the time goes:
time: 443 us; the launch traced here: 438 us
  matrix products  162 us (37%)
  waiting for transfers between devices  127 us (29%)
  loops' own time  40.8 us (9%)
  blocking collectives  38.4 us (9%)
  other arithmetic  27.1 us (6%)
  local copies, waits for them, and re-layouts  25.4 us (6%)
  between operations  13.7 us (3%)
    all_gather x1, waiting for transfers between devices, in_one_piece(): lax.all_gather(both, axis, axis=dim, tiled=True)  111 us
    dot_general x32, matrix products, block_keys(): jnp.einsum('kr,rhd->khd', latent_rows, value_up, preferred_element_type=j...  42.9 us
    dot_general x32, matrix products, block_keys(): jnp.einsum('kr,rhd->khd', latent_rows, key_up, preferred_element_type=jnp...  42.7 us
    dot_general x32, matrix products, attend(): jnp.einsum('qhr,kr->hqk', query_rot, rotated_rows, preferred_element_type...  41.3 us
    all_to_all x2, blocking collectives, sent_and_summed(): tiles = lax.all_to_all(cut_along(x, dim, devices), axis, 0, 0, tiled=True)  38.4 us
    another operation x1, loops' own time, fold_piece(): return lax.fori_loop(0, count // block, one_block, carry)  20.3 us
    another operation x16, loops' own time, one_block(): return lax.cond(first_key <= last_all, work, lambda inner: inner, state)  19.6 us
    all_to_all x1, waiting for transfers between devices, sent_to_all(): lax.all_to_all(jnp.broadcast_to(x[None], (devices, *x.shape)), axis, 0, 0...  15.8 us
  transfers between devices with their start and end apart: 3, of which 2 were waited for; matrix products, arithmetic and copies ran while one was open for 46% of the time, Pallas kernels for 0%

commit v1 on v0

v1 whole, which is shorter than its diff:
```python
import functools

import jax
import jax.numpy as jnp
from jax import lax
from jax.experimental import pallas as pl
from jax.experimental.pallas import tpu as pltpu
from jax.sharding import PartitionSpec as P

MESH = pl.DeviceIdType.MESH
THETA = 10000.0
EPS = 1e-06
NEGATIVE = -1e30
LOG2E = 1.4426950408889634
RING = 8
LAG = 3
F32 = jnp.float32
BF16 = jnp.bfloat16

HALF = 128
PIECE = HALF + 16


def rem(v, n):
    return lax.rem(v, jnp.int32(n))


def div(v, n):
    return lax.div(v, jnp.int32(n))


def kernel(
    pieces, queries, kb, kl, vb, vl, ob, ol, resid, again, mgain, gate_w, up_w, down_w,
    out,
    lat, wts, wout, rows, att, qt, kup, vupt, spread, peak, total, accum, att_t, hs, norm, hid, part, pbuf, sbuf, rbuf, wown,
    l_recv, l_first, l_plus, l_minus, p_recv, p_send,
    w_recv, w_first, w_plus, w_minus,
    loc, o_send, o_recv, r_send, r_recv, a_send, a_recv, s_send, s_recv,
):
    sp = lax.axis_index("sp")
    tp = lax.axis_index("tp")
    core = rem(tp, 2)
    xx = div(tp, 2)
    other = 1 - core
    sa = 1 + 7 * core
    sb = 8 - 7 * core
    a = rem(lax.div(sp, sa), RING)
    b = rem(lax.div(sp, sb), RING)

    def at(first, second):
        return rem(first + 16, RING) * sa + rem(second + 16, RING) * sb

    def turned(first, second):
        return rem(first + 16, RING) * sb + rem(second + 16, RING) * sa

    def rel(k):
        return div(k + 1, 2) * (1 - 2 * rem(k, 2))

    a_up, a_dn, b_up, b_dn = (
        (at(a + 1, b), tp), (at(a - 1, b), tp), (at(a, b + 1), tp), (at(a, b - 1), tp)
    )
    partner = (sp, 2 * xx + other)

    def across(step):
        return 2 * rem(xx + step, 4) + core

    x_up, x_far, x_dn = (sp, across(1)), (sp, across(2)), (sp, across(3))

    def remote(src, dst, ssem, rsem, dev):
        return pltpu.make_async_remote_copy(
            src_ref=src, dst_ref=dst, send_sem=ssem, recv_sem=rsem, device_id=dev, device_id_type=MESH
        )

    own_b = pltpu.make_async_copy(ob, wout.at[tp, pl.ds(0, 128)], loc.at[0])
    own_l = pltpu.make_async_copy(ol, wout.at[tp, pl.ds(128, 64)], loc.at[1])
    own_r = pltpu.make_async_copy(resid, rows.at[tp], loc.at[2])
    own_b.start()
    own_l.start()
    own_r.start()

    barrier = pltpu.get_barrier_semaphore()
    for dev in (a_up, a_dn, b_up, b_dn, partner, x_up, x_far, x_dn):
        pl.semaphore_signal(barrier, inc=1, device_id=dev, device_id_type=MESH)
    pl.semaphore_wait(barrier, 8)

    class Stream:
        def __init__(self, own, slot, recv, first, plus, minus, push):
            self.own, self.slot, self.recv = own, slot, recv
            self.first, self.plus, self.minus, self.push = first, plus, minus, push

        def send(self, src, o, ssem, dev):
            return remote(src, self.slot(o), ssem, self.recv.at[o], dev)

        def start(self):
            for index, dev in ((0, a_up), (7, a_dn)):
                self.send(self.own, sp, self.first.at[index], dev).start()
            self.send(self.own, sp, self.plus.at[0], b_up).start()
            self.send(self.own, sp, self.minus.at[0], b_dn).start()

        def arrived(self, o):
            self.send(self.slot(o), o, self.first.at[0], partner).wait_recv()

        def near(self, k):
            o = at(a + rel(k), b)
            self.arrived(o)

            @pl.when((rem(k, 2) == 1) & (k < 7))
            def _():
                self.send(self.slot(o), o, self.first.at[k], a_up).start()

            @pl.when((rem(k, 2) == 0) & (k < 6))
            def _():
                self.send(self.slot(o), o, self.first.at[k], a_dn).start()

            self.send(self.slot(o), o, self.plus.at[k], b_up).start()
            self.send(self.slot(o), o, self.minus.at[k], b_dn).start()
            if self.push:
                self.give(o)

        def give(self, o):
            remote(self.slot(o), self.slot(o), p_send.at[o], p_recv.at[o], partner).start()

        def far(self, n):
            kp, km, d = ring_step(n)
            op, om = at(a + rel(kp), b - d), at(a + rel(km), b + d)
            self.arrived(op)

            @pl.when(n < 28)
            def _():
                self.send(self.slot(op), op, self.plus.at[n], b_up).start()

            if self.push:
                self.give(op)
            self.arrived(om)

            @pl.when((n < 24) | ((n >= 28) & (n < 32)))
            def _():
                self.send(self.slot(om), om, self.minus.at[n], b_dn).start()

            if self.push:
                self.give(om)

        def step(self, n):
            @pl.when((n >= 1) & (n < 8))
            def _():
                self.near(n)

            @pl.when((n >= 8) & (n < 36))
            def _():
                self.far(n)

        def drain(self):
            def sent(sem):
                remote(self.slot(sp), self.slot(sp), sem, self.recv.at[sp], partner).wait_send()

            for index in (0, 1, 2, 3, 4, 5, 7):
                sent(self.first.at[index])

            @pl.loop(0, 28)
            def _(n):
                sent(self.plus.at[n])

            @pl.loop(0, 24)
            def _(n):
                sent(self.minus.at[n])

            @pl.loop(28, 32)
            def _(n):
                sent(self.minus.at[n])

    def ring_step(n):
        last = div(n, 32)
        kp = rem(n, 8)
        return kp, kp + 4 * last, div(n, 8)

    latents = Stream(
        pieces.at[core], lambda o: lat.at[core, o], l_recv, l_first, l_plus, l_minus, True
    )
    weights = Stream(wown, lambda o: wts.at[o], w_recv, w_first, w_plus, w_minus, False)
    latents.start()

    own_r.wait()
    for i, dev in enumerate((partner, x_up, x_dn, x_far)):
        remote(rows.at[tp], rows.at[tp], r_send.at[i], r_recv.at[tp], dev).start()
    own_b.wait()
    own_l.wait()
    for i, dev in enumerate((partner, x_up, x_dn)):
        remote(wout.at[tp], wout.at[tp], o_send.at[i], o_recv.at[tp], dev).start()

    def share_rows():
        for i in (1, 2, 3):
            t = across(i)
            remote(rows.at[t], rows.at[t], r_send.at[3 + i], r_recv.at[t], partner).wait_recv()
            remote(rows.at[t], rows.at[t], r_send.at[3 + i], r_recv.at[t], partner).start()

    top, low = pl.ds(0, 96), pl.ds(96, 96)

    def share_near():
        for i, t, rest, dev in ((3, across(3), top, x_up), (4, across(1), low, x_dn)):
            remote(wout.at[t], wout.at[t], o_send.at[i], o_recv.at[t], partner).wait_recv()
            far = 8 if i == 3 else 9
            remote(wout.at[t, rest], wout.at[t, rest], o_send.at[i], o_recv.at[far], dev).start()
            remote(wout.at[t], wout.at[t], o_send.at[i + 2], o_recv.at[t], partner).start()

    def share_far():
        t = across(2)
        for i, rest in ((8, top), (9, low)):
            remote(wout.at[t, rest], wout.at[t, rest], o_send.at[0], o_recv.at[i], partner).wait_recv()
            remote(wout.at[t, rest], wout.at[t, rest], o_send.at[i - 1], o_recv.at[i + 2], partner).start()

    qt[...] = queries[...].T
    kup[...] = jnp.zeros_like(kup)
    kup[:, 0:128] = kb[...]
    kup[:, 128:192] = kl[...]
    vupt[0:128, :] = vb[...].T
    vupt[128:192, :] = vl[...].T
    spread[...] = (
        lax.broadcasted_iota(jnp.int32, (32, 256), 1) == lax.broadcasted_iota(jnp.int32, (32, 256), 0) + 192
    ).astype(F32).astype(BF16)
    wown[...] = jnp.zeros_like(wown)
    wown[:, 0:352] = gate_w[...]
    wown[:, 384:736] = up_w[...]
    wown[:, 768:1120] = down_w[...].T

    column = lax.broadcasted_iota(jnp.int32, (1, 512), 1)
    factor = jnp.where(column < 256, LOG2E * 160 ** (-0.5), LOG2E * 96 ** (-0.5)).astype(F32)

    def project(halves):
        rows_of = jnp.concatenate([h[0:HALF, :] for h in halves], axis=0)
        turned_rot = jnp.concatenate(
            [
                jnp.concatenate([h[HALF:PIECE, 0:HALF] for h in halves], axis=1),
                jnp.concatenate([h[HALF:PIECE, HALF:256] for h in halves], axis=1),
            ],
            axis=0,
        )
        keys = jnp.dot(rows_of, kup[...], preferred_element_type=F32) + lax.dot_general(
            turned_rot, spread[...], (((0,), (0,)), ((), ())), preferred_element_type=F32
        )
        values = lax.dot_general(
            vupt[...], rows_of, (((1,), (1,)), ((), ())), preferred_element_type=F32
        )
        return keys.astype(BF16), values.astype(BF16)

    def fold(halves, blocks):
        keys, values = project(halves)
        scores = jnp.dot(keys, qt[...], preferred_element_type=F32) * factor
        if blocks is None:
            seen = lax.broadcasted_iota(jnp.int32, scores.shape, 0) <= (
                lax.broadcasted_iota(jnp.int32, scores.shape, 1) & 255
            )
            scores = jnp.where(seen, scores, NEGATIVE)
        else:
            scores = jnp.concatenate(
                [
                    scores[i * HALF : (i + 1) * HALF] + jnp.where(o <= sp, 0.0, NEGATIVE).astype(F32)
                    for i, o in enumerate(blocks)
                ],
                axis=0,
            )
        old = peak[...]
        new = jnp.maximum(old, jnp.max(scores, axis=0, keepdims=True))
        shrink = jnp.exp2(old - new)
        wt = jnp.exp2(scores - new)
        peak[...] = new
        total[...] = total[...] * shrink + jnp.sum(wt, axis=0, keepdims=True)
        wt = wt.astype(BF16)
        accum[0:128, :] = accum[0:128, :] * shrink[:, 0:256] + jnp.dot(
            values[0:128], wt[:, 0:256], preferred_element_type=F32
        )
        accum[128:192, :] = accum[128:192, :] * shrink[:, 256:512] + jnp.dot(
            values[128:192], wt[:, 256:512], preferred_element_type=F32
        )

    peak[...] = jnp.full_like(peak, NEGATIVE)
    total[...] = jnp.zeros_like(total)
    accum[...] = jnp.zeros_like(accum)
    fold([pieces.at[0], pieces.at[1]], None)

    def given(o):
        remote(lat.at[other, o], lat.at[other, o], p_send.at[0], p_recv.at[o], partner).wait_recv()

    def compute(n):
        @pl.when((n >= 1) & (n < 8))
        def _():
            o1, o2 = at(a + rel(n), b), turned(b + rel(n), a)
            given(o2)

            @pl.when(jnp.minimum(o1, o2) <= sp)
            def _():
                fold([lat.at[core, o1], lat.at[other, o2]], (o1, o2))

        @pl.when((n >= 8) & (n < 36))
        def _():
            kp, km, d = ring_step(n)
            o1, o2 = at(a + rel(kp), b - d), at(a + rel(km), b + d)
            o3, o4 = turned(b + rel(kp), a - d), turned(b + rel(km), a + d)
            given(o3)
            given(o4)

            @pl.when(jnp.minimum(jnp.minimum(o1, o2), jnp.minimum(o3, o4)) <= sp)
            def _():
                fold(
                    [lat.at[core, o1], lat.at[core, o2], lat.at[other, o3], lat.at[other, o4]],
                    (o1, o2, o3, o4),
                )

    @pl.loop(1, 36 + LAG)
    def _(n):
        latents.step(n)

        @pl.when(n == 36)
        def _():
            weights.start()

        @pl.when(n >= 37)
        def _():
            weights.step(n - 36)

        @pl.when(n == 20)
        def _():
            share_rows()

        @pl.when(n == 28)
        def _():
            share_near()

        compute(n - LAG)

    result = accum[...]
    att[tp, 0:128, :] = (result[0:128] / total[:, 0:256]).astype(BF16)
    att[tp, 128:192, :] = (result[128:192] / total[:, 256:512]).astype(BF16)

    weights.step(jnp.int32(LAG))

    for i, dev in enumerate((x_far, x_up, x_dn, partner)):
        remote(att.at[tp], att.at[tp], a_send.at[i], a_recv.at[tp], dev).start()

    @pl.loop(LAG + 1, 8)
    def _(n):
        weights.step(n)

    share_far()
    for i in (1, 3, 2):
        t = across(i)
        remote(att.at[t], att.at[t], a_send.at[0], a_recv.at[t], partner).wait_recv()
        remote(att.at[t], att.at[t], a_send.at[3 + i], a_recv.at[t], partner).start()

    @pl.loop(8, 10)
    def _(n):
        weights.step(n)

    for i in (0, 1, 2, 3):
        t = 2 * rem(xx + i, 4) + other
        remote(att.at[t], att.at[t], a_send.at[0], a_recv.at[t], partner).wait_recv()
        remote(rows.at[t], rows.at[t], r_send.at[0], r_recv.at[t], partner).wait_recv()
        if i == 2:
            for j, rest in ((10, top), (11, low)):
                remote(wout.at[t, rest], wout.at[t, rest], o_send.at[0], o_recv.at[j], partner).wait_recv()
        else:
            remote(wout.at[t], wout.at[t], o_send.at[0], o_recv.at[t], partner).wait_recv()

    @pl.loop(0, 8)
    def _(t):
        att_t[t] = att[t].T

    @pl.loop(0, 8)
    def _(j):
        cols = pl.ds(pl.multiple_of(j * 256, 256), 256)
        acc = jnp.dot(att_t[0], wout[0, :, cols], preferred_element_type=F32)
        for t in range(1, 8):
            acc = acc + jnp.dot(att_t[t], wout[t, :, cols], preferred_element_type=F32)
        hs[:, cols] = acc
        weights.step(10 + j)

    for i in range(7):
        remote(rows.at[tp], rows.at[tp], r_send.at[i], r_recv.at[tp], partner).wait_send()

    @pl.loop(0, 8)
    def _(t):
        chunk = pl.ds(pl.multiple_of(t * 32, 32), 32)
        value = hs[chunk, :]
        scale = lax.rsqrt(jnp.mean(value * value, axis=-1, keepdims=True) + EPS)
        mixed = (rows[t].astype(F32) + value * scale * again[...]).astype(BF16)
        rows[t] = mixed
        value = mixed.astype(F32)
        scale = lax.rsqrt(jnp.mean(value * value, axis=-1, keepdims=True) + EPS)
        norm[chunk, :] = (value * scale * mgain[...]).astype(BF16)
        weights.step(18 + t)

    @pl.loop(26, 36)
    def _(n):
        weights.step(n)

    wts[sp] = wown[...]
    both = jnp.dot(norm[...], wts[:, :, 0:768].reshape(2048, 768), preferred_element_type=F32)
    gate, up = both[:, 0:384], both[:, 384:768]
    hid[...] = (gate / (1.0 + jnp.exp(-gate)) * up).astype(BF16)

    @pl.loop(0, 8)
    def _(j):
        down = wts[pl.ds(j * 8, 8), :, 768:1152].reshape(256, 384)
        value = lax.dot_general(hid[...], down, (((1,), (1,)), ((), ())), preferred_element_type=F32)
        part[:, :, pl.ds(pl.multiple_of(j * 256, 256), 256)] = value.astype(BF16).reshape(8, 32, 256)

    latents.drain()

    @pl.loop(0, 64)
    def _(o):
        @pl.when(o != sp)
        def _():
            remote(lat.at[core, o], lat.at[core, o], p_send.at[o], p_recv.at[o], partner).wait_send()

    for i in (2, 1, 3, 0):
        x_to = rem(xx + i, 4)
        remote(part.at[2 * x_to + other], pbuf.at[x_to], s_send.at[i], s_recv.at[i], partner).start()
    ready = None
    for i, dev in ((2, x_far), (1, x_up), (3, x_dn)):
        x_to = rem(xx + i, 4)
        remote(pbuf.at[x_to], pbuf.at[x_to], s_send.at[i], s_recv.at[i], partner).wait_recv()
        sbuf[i - 1] = (part[2 * x_to + core].astype(F32) + pbuf[x_to].astype(F32)).astype(BF16)
        if ready is not None:
            ready.start()
        ready = remote(sbuf.at[i - 1], rbuf.at[i - 1], s_send.at[3 + i], s_recv.at[3 + i], dev)
    remote(pbuf.at[xx], pbuf.at[xx], s_send.at[0], s_recv.at[0], partner).wait_recv()
    summed = part[tp].astype(F32) + pbuf[xx].astype(F32)
    ready.start()
    weights.drain()
    for i in (1, 3, 2):
        remote(rbuf.at[i - 1], rbuf.at[i - 1], s_send.at[3 + i], s_recv.at[3 + i], partner).wait_recv()
        summed = summed + rbuf[i - 1].astype(F32)
    out[...] = (rows[tp].astype(F32) + 0.5 * summed).astype(BF16)

    for i in range(7):
        remote(att.at[tp], att.at[tp], a_send.at[i], a_recv.at[tp], partner).wait_send()
        remote(rbuf.at[0], rbuf.at[0], s_send.at[i], s_recv.at[i], partner).wait_send()
    for i in (0, 1, 2, 5, 6):
        remote(wout.at[tp], wout.at[tp], o_send.at[i], o_recv.at[tp], partner).wait_send()
    for i in (3, 4, 7, 8):
        remote(wout.at[tp, top], wout.at[tp, top], o_send.at[i], o_recv.at[tp], partner).wait_send()


def rotate(values, cosine, sine):
    first, second = values[:, :16], values[:, 16:]
    return jnp.concatenate([first * cosine - second * sine, first * sine + second * cosine], axis=-1)


def shards(
    residual_in, query_lean, query_broad, latent, rope_key, latent_gain, key_up_lean, key_up_broad, value_up_lean,
    value_up_broad, out_lean, out_broad, attn_gain, mlp_gain, gate_weight, up_weight, down_weight,
):
    tokens = latent.shape[0]
    positions = lax.axis_index("sp") * tokens + jnp.arange(tokens, dtype=jnp.int32)
    freqs = THETA ** (-2.0 * jnp.arange(16, dtype=F32) / 32)
    angle = positions.astype(F32)[:, None] * freqs[None, :]
    cosine, sine = jnp.cos(angle), jnp.sin(angle)

    def rounded(v):
        return rotate(v.astype(F32), cosine, sine).astype(BF16)

    wide = latent.astype(F32)
    normed = (
        wide * lax.rsqrt(jnp.mean(wide * wide, axis=-1, keepdims=True) + EPS) * latent_gain
    ).astype(BF16)
    rot = rounded(rope_key)
    turned = rot.reshape(2, HALF, 2, 16).transpose(0, 3, 2, 1).reshape(2, 16, 256)
    pieces = jnp.concatenate([normed.reshape(2, HALF, 256), turned], axis=1)
    broad, lean = query_broad[:, 0], query_lean[:, 0]
    pad = functools.partial(jnp.zeros, dtype=BF16)
    queries = jnp.concatenate(
        [
            jnp.concatenate([broad[:, :128], pad((tokens, 64)), rounded(broad[:, 128:]), pad((tokens, 32))], axis=1),
            jnp.concatenate([pad((tokens, 128)), lean[:, :64], rounded(lean[:, 64:]), pad((tokens, 32))], axis=1),
        ],
        axis=0,
    )
    vmem = pl.BlockSpec(memory_space=pltpu.VMEM)
    hbm = pl.BlockSpec(memory_space=pl.ANY)
    sems = pltpu.SemaphoreType.DMA
    scratch = [
        pltpu.VMEM((2, 64, PIECE, 256), BF16),
        pltpu.VMEM((64, 32, 1152), BF16),
        pltpu.VMEM((8, 192, 2048), BF16),
        pltpu.VMEM((8, 32, 2048), BF16),
        pltpu.VMEM((8, 192, 256), BF16),
        pltpu.VMEM((256, 512), BF16),
        pltpu.VMEM((256, 256), BF16),
        pltpu.VMEM((192, 256), BF16),
        pltpu.VMEM((32, 256), BF16),
        pltpu.VMEM((1, 512), F32),
        pltpu.VMEM((1, 512), F32),
        pltpu.VMEM((192, 256), F32),
        pltpu.VMEM((8, 256, 192), BF16),
        pltpu.VMEM((256, 2048), F32),
        pltpu.VMEM((256, 2048), BF16),
        pltpu.VMEM((256, 384), BF16),
        pltpu.VMEM((8, 32, 2048), BF16),
        pltpu.VMEM((4, 32, 2048), BF16),
        pltpu.VMEM((3, 32, 2048), BF16),
        pltpu.VMEM((3, 32, 2048), BF16),
        pltpu.VMEM((32, 1152), BF16),
        sems((64,)), sems((8,)), sems((28,)), sems((32,)), sems((64,)), sems((64,)),
        sems((64,)), sems((8,)), sems((28,)), sems((32,)),
        sems((3,)), sems((9,)), sems((12,)), sems((7,)), sems((8,)), sems((7,)), sems((8,)), sems((7,)), sems((7,)),
    ]
    return pl.pallas_call(
        kernel,
        out_shape=jax.ShapeDtypeStruct((32, 2048), BF16),
        in_specs=[vmem] * 6 + [hbm] * 3 + [vmem] * 5,
        out_specs=vmem,
        scratch_shapes=scratch,
        compiler_params=pltpu.CompilerParams(
            collective_id=0, has_side_effects=True, vmem_limit_bytes=60 * 1024 * 1024
        ),
    )(
        pieces, queries, key_up_broad[:, 0], key_up_lean[:, 0], value_up_broad[:, 0], value_up_lean[:, 0],
        out_broad[0], out_lean[0], residual_in, attn_gain[None], mlp_gain[None], gate_weight, up_weight, down_weight,
    )


def solution(mesh):
    in_specs = (
        P(("sp", "tp"), None), P("sp", "tp", None), P("sp", "tp", None), P("sp", None), P("sp", None), P(),
        P(None, "tp", None), P(None, "tp", None), P(None, "tp", None), P(None, "tp", None),
        P("tp", None, None), P("tp", None, None), P(), P(), P("sp", "tp"), P("sp", "tp"), P("tp", "sp"),
    )
    return jax.shard_map(
        shards, mesh=mesh, in_specs=in_specs, out_specs=P(("sp", "tp"), None), check_vma=False
    )
```

time: 443 us -> 125 us (0.28)
  the two profiles are of different devices: /device:TPU:480 before, /device:TPU:1 now
where the time goes in v1:
time: 125 us
  Pallas kernels  114 us (91%)
  local copies, waits for them, and re-layouts  6.99 us (6%)
  other arithmetic  2.91 us (2%)
    pallas_call x1, Pallas kernels, shards(): pl.pallas_call(kernel, out_shape=jax.ShapeDtypeStruct((32, 2048), BF16),...  114 us
    unnamed x21, local copies, waits for them, and re-layouts  6.43 us

profile of v1, /device:TPU:1, one launch (start us, length us, event | category | flops | bytes accessed | tf_op | source)
XLA Modules:
  0.0 124.5 jit_solution(17169120946339583344)
XLA Ops:
  0.0 0.0 copy-start.1
  0.0 1.0 copy.47
  1.0 0.0 copy-done.1
  1.0 0.1 copy.48
  1.1 0.1 slice_convert_fusion
  1.3 0.6 fusion.20
  1.9 0.2 concatenate.24
  2.1 0.2 concatenate.25
  2.3 0.0 copy-start.5
  2.3 0.7 pad_maximum_fusion.queries
  3.0 0.0 copy-done.5
  3.0 0.1 copy.42
  3.1 0.6 fusion.15
  3.7 0.0 copy-start
  3.7 0.1 copy.44
  3.8 0.1 copy.45
  4.0 0.7 copy-done
  4.6 0.1 fusion
  4.7 0.0 copy-start.6
  4.8 0.7 copy-done.6
  5.4 0.1 fusion.2
  5.5 0.0 copy-start.4
  5.5 0.7 pad_maximum_fusion.1.pieces
  6.2 0.1 copy-done.4
  6.3 0.0 copy-start.2
  6.3 0.7 copy.51.down_w
  7.0 0.0 copy-done.2
  7.0 0.7 copy.49
  7.8 0.0 copy-done.3
  7.8 0.7 copy.50
  8.5 114.4 %shard_map.163 = bf16[32,2048]{1,0:T(8,128)(2,1)} custom-call(bf16[2,144,256]{2,1,0:T(8,128)(2,1)} %pad_maximum_fusion.1.pieces, bf16[512,256]{1,0:T(8,128)(2,1)} %pad_maximum_fusion.queries, bf16[256,128]{1,0:T(8,128)(2,1)} %bitcast.24, bf16[256,64]{1,0:T(8,128)(2,1)} %bitcast.22, bf16[256,128]{1,0:T(8,128)(2,1)} %bitcast.25, bf16[256,64]{1,0:T(8,128)(2,1)} %bitcast.23, ...), custom_call_target="tpu_custom_call" | custom-call | tf_op jit(solution)/shard_map/pallas_call | solution.py:506
  123.0 1.6 %copy.53 = bf16[32,2048]{1,0:T(8,128)(2,1)} copy(bf16[32,2048]{1,0:T(8,128)(2,1)} %shard_map.163) | data formatting | bytes 262144
  (13 shorter events, 0.1 us)
Async XLA Ops:
  0.0 1.0 copy-start.1
  2.3 0.7 copy-start.5
  3.7 0.9 copy-start
  4.7 0.7 copy-start.6
  5.5 0.7 copy-start.4
  6.3 0.8 copy-start.2
  7.0 0.8 copy-start.3

commit v2 on v1

v2 whole, which is shorter than its diff:
```python
import jax
import jax.numpy as jnp
from jax import lax
from jax.experimental import pallas as pl
from jax.experimental.pallas import tpu as pltpu
from jax.sharding import PartitionSpec as P

MESH = pl.DeviceIdType.MESH
THETA = 10000.0
EPS = 1e-06
NEGATIVE = -1e30
LOG2E = 1.4426950408889634
RING = 8
F32 = jnp.float32
BF16 = jnp.bfloat16

HALF = 128
PIECE = HALF + 16


def rem(v, n):
    return lax.rem(v, jnp.int32(n))


def div(v, n):
    return lax.div(v, jnp.int32(n))


def kernel(
    latent, lgain, rope, qb, ql, cosine, sine, kb, kl, vb, vl, ob, ol, resid, again, mgain, gate_w, up_w, down_w,
    out,
    pieces, score, value, most, lat, wts, wout, rows, att, qt, kup, vupt, spread, peak, total, accum, att_t, hs, norm, hid, part, pbuf, sbuf, rbuf, wown,
    l_recv, w_recv, p_recv, first, plus, minus, p_send,
    loc, o_send, o_recv, r_send, r_recv, a_send, a_recv, s_send, s_recv,
):
    sp = lax.axis_index("sp")
    tp = lax.axis_index("tp")
    core = rem(tp, 2)
    xx = div(tp, 2)
    other = 1 - core
    sa = 1 + 7 * core
    sb = 8 - 7 * core
    a = rem(lax.div(sp, sa), RING)
    b = rem(lax.div(sp, sb), RING)

    def at(i, j):
        return rem(i + 16, RING) * sa + rem(j + 16, RING) * sb

    def turned(i, j):
        return rem(i + 16, RING) * sb + rem(j + 16, RING) * sa

    def rel(k):
        return div(k + 1, 2) * (1 - 2 * rem(k, 2))

    a_up, a_dn, b_up, b_dn = (
        (at(a + 1, b), tp), (at(a - 1, b), tp), (at(a, b + 1), tp), (at(a, b - 1), tp)
    )
    partner = (sp, 2 * xx + other)

    def across(step):
        return 2 * rem(xx + step, 4) + core

    x_up, x_far, x_dn = (sp, across(1)), (sp, across(2)), (sp, across(3))

    def remote(src, dst, ssem, rsem, dev):
        return pltpu.make_async_remote_copy(
            src_ref=src, dst_ref=dst, send_sem=ssem, recv_sem=rsem, device_id=dev, device_id_type=MESH
        )

    own_b = pltpu.make_async_copy(ob, wout.at[tp, pl.ds(0, 128)], loc.at[0])
    own_l = pltpu.make_async_copy(ol, wout.at[tp, pl.ds(128, 64)], loc.at[1])
    own_r = pltpu.make_async_copy(resid, rows.at[tp], loc.at[2])
    own_b.start()
    own_l.start()
    own_r.start()

    barrier = pltpu.get_barrier_semaphore()
    for dev in (a_up, a_dn, b_up, b_dn, partner, x_up, x_far, x_dn):
        pl.semaphore_signal(barrier, inc=1, device_id=dev, device_id_type=MESH)

    def rotated(ref, start):
        low, high = ref[start : start + 16, :].astype(F32), ref[start + 16 : start + 32, :].astype(F32)
        co, si = cosine[...], sine[...]
        return (low * co - high * si).astype(BF16), (low * si + high * co).astype(BF16)

    wide = latent[...].astype(F32)
    wide = (wide * lax.rsqrt(jnp.mean(wide * wide, axis=-1, keepdims=True) + EPS) * lgain[...]).astype(BF16)
    low, high = rotated(rope, 0)
    for h in range(2):
        pieces[h, 0:HALF, :] = wide[h * HALF : (h + 1) * HALF]
        pieces[h, HALF:PIECE, 0:HALF] = low[:, h * HALF : (h + 1) * HALF]
        pieces[h, HALF:PIECE, HALF:256] = high[:, h * HALF : (h + 1) * HALF]
    qt[...] = jnp.zeros_like(qt)
    qt[0:128, 0:256] = qb[0:128, :]
    qt[128:192, 256:512] = ql[0:64, :]
    for ref, start, at_column in ((qb, 128, 0), (ql, 64, 256)):
        low, high = rotated(ref, start)
        qt[192:208, at_column : at_column + 256] = low
        qt[208:224, at_column : at_column + 256] = high

    pl.semaphore_wait(barrier, 8)

    class Stream:
        def __init__(self, own, slot, pair, recv, fresh):
            self.own, self.slot, self.pair, self.recv, self.fresh = own, slot, pair, recv, fresh

        def go(self, src, o, ssem, n, dev):
            remote(src, self.slot(o), ssem, self.recv.at[n], dev).start()

        def free(self, sem, when=True):
            if when is True:
                remote(self.slot(0), self.slot(0), sem, self.recv.at[0], partner).wait_send()
            else:
                pl.when(when)(lambda: self.free(sem))

        def start(self):
            for index, n, dev in ((0, 1, a_up), (7, 2, a_dn)):
                if not self.fresh:
                    self.free(first.at[index])
                self.go(self.own, sp, first.at[index], n, dev)

        def spread(self, k, src=None):
            o = at(a + rel(k), b)
            src = self.slot(o) if src is None else src
            for sems, dev in ((plus, b_up), (minus, b_dn)):
                if not self.fresh:
                    self.free(sems.at[k])
                self.go(src, o, sems.at[k], k + 8, dev)

        def near(self, k):
            o = at(a + rel(k), b)
            remote(self.slot(o), self.slot(o), first.at[0], self.recv.at[k], partner).wait_recv()

            @pl.when((rem(k, 2) == 1) & (k < 7))
            def _():
                if not self.fresh:
                    self.free(first.at[k])
                self.go(self.slot(o), o, first.at[k], k + 2, a_up)

            @pl.when((rem(k, 2) == 0) & (k < 6))
            def _():
                if not self.fresh:
                    self.free(first.at[k])
                self.go(self.slot(o), o, first.at[k], k + 2, a_dn)

        def far(self, n):
            kp, km, d = ring_step(n)
            k = rem(n, 8)
            op, om = at(a + rel(kp), b - d), at(a + rel(km), b + d)
            remote(self.pair, self.pair, first.at[0], self.recv.at[n], partner).wait_recv()

            @pl.when(n < 28)
            def _():
                self.free(plus.at[k])
                self.go(self.slot(op), op, plus.at[k], n + 8, b_up)

            @pl.when((n < 24) | ((n >= 28) & (n < 32)))
            def _():
                self.free(minus.at[k])
                self.go(self.slot(om), om, minus.at[k], jnp.where(n < 24, n + 8, n + 4), b_dn)

            return k, op, om

    def give(n, o):
        remote(lat.at[core, o], lat.at[core, o], p_send.at[rem(n, 8)], p_recv.at[n], partner).start()

    two = lat.at[0, pl.ds(0, 2)]

    def given_free(n, count):
        ref = two if count == 2 else lat.at[0, 0]
        remote(ref, ref, p_send.at[rem(n, 8)], p_recv.at[0], partner).wait_send()

    def ring_step(n):
        last = div(n, 32)
        kp = rem(n, 8)
        return kp, kp + 4 * last, div(n, 8)

    latents = Stream(pieces.at[core], lambda o: lat.at[core, o], two, l_recv, True)
    weights = Stream(wown, lambda o: wts.at[o], wts.at[pl.ds(0, 2)], w_recv, False)

    def latent_near(k):
        latents.near(k)
        latents.spread(k)
        give(k, at(a + rel(k), b))

    def latent_far(n):
        k, op, om = latents.far(n)

        @pl.when(n >= 16)
        def _():
            given_free(n, 2)

        @pl.when((n > 8) & (n < 16))
        def _():
            given_free(n, 1)

        give(n, op)
        give(n, om)

    latents.start()
    latents.spread(jnp.int32(0), pieces.at[core])

    own_r.wait()
    for i, dev in enumerate((partner, x_up, x_dn, x_far)):
        remote(rows.at[tp], rows.at[tp], r_send.at[i], r_recv.at[tp], dev).start()
    own_b.wait()
    own_l.wait()
    for i, dev in enumerate((partner, x_up, x_dn)):
        remote(wout.at[tp], wout.at[tp], o_send.at[i], o_recv.at[tp], dev).start()

    def share_rows():
        for i in (1, 2, 3):
            t = across(i)
            remote(rows.at[t], rows.at[t], r_send.at[3 + i], r_recv.at[t], partner).wait_recv()
            remote(rows.at[t], rows.at[t], r_send.at[3 + i], r_recv.at[t], partner).start()

    top, low = pl.ds(0, 96), pl.ds(96, 96)

    def share_near():
        for i, t, rest, dev in ((3, across(3), top, x_up), (4, across(1), low, x_dn)):
            remote(wout.at[t], wout.at[t], o_send.at[i], o_recv.at[t], partner).wait_recv()
            far = 8 if i == 3 else 9
            remote(wout.at[t, rest], wout.at[t, rest], o_send.at[i], o_recv.at[far], dev).start()
            remote(wout.at[t], wout.at[t], o_send.at[i + 2], o_recv.at[t], partner).start()

    def share_far():
        t = across(2)
        for i, rest in ((8, top), (9, low)):
            remote(wout.at[t, rest], wout.at[t, rest], o_send.at[0], o_recv.at[i], partner).wait_recv()
            remote(wout.at[t, rest], wout.at[t, rest], o_send.at[i - 1], o_recv.at[i + 2], partner).start()

    kup[...] = jnp.zeros_like(kup)
    kup[:, 0:128] = kb[...]
    kup[:, 128:192] = kl[...].T
    vupt[0:128, :] = vb[...].T
    vupt[128:192, :] = vl[...]
    spread[...] = (
        lax.broadcasted_iota(jnp.int32, (32, 256), 1) == lax.broadcasted_iota(jnp.int32, (32, 256), 0) + 192
    ).astype(F32).astype(BF16)
    wown[...] = jnp.zeros_like(wown)
    wown[:, 0:352] = gate_w[...]
    wown[:, 384:736] = up_w[...]
    wown[:, 768:1120] = down_w[...]

    column = lax.broadcasted_iota(jnp.int32, (1, 512), 1)
    factor = jnp.where(column < 256, LOG2E * 160 ** (-0.5), LOG2E * 96 ** (-0.5)).astype(F32)

    def project(halves):
        rows_of = jnp.concatenate([h[0:HALF, :] for h in halves], axis=0)
        turned_rot = jnp.concatenate(
            [
                jnp.concatenate([h[HALF:PIECE, 0:HALF] for h in halves], axis=1),
                jnp.concatenate([h[HALF:PIECE, HALF:256] for h in halves], axis=1),
            ],
            axis=0,
        )
        keys = jnp.dot(rows_of, kup[...], preferred_element_type=F32) + lax.dot_general(
            turned_rot, spread[...], (((0,), (0,)), ((), ())), preferred_element_type=F32
        )
        values = lax.dot_general(
            vupt[...], rows_of, (((1,), (1,)), ((), ())), preferred_element_type=F32
        )
        return keys.astype(BF16), values.astype(BF16)

    def fold(halves, blocks):
        keys, values = project(halves)
        scores = jnp.dot(keys, qt[...], preferred_element_type=F32) * factor
        if blocks is None:
            seen = lax.broadcasted_iota(jnp.int32, scores.shape, 0) <= (
                lax.broadcasted_iota(jnp.int32, scores.shape, 1) & 255
            )
            scores = jnp.where(seen, scores, NEGATIVE)
        else:
            scores = jnp.concatenate(
                [
                    scores[i * HALF : (i + 1) * HALF] + jnp.where(o <= sp, 0.0, NEGATIVE).astype(F32)
                    for i, o in enumerate(blocks)
                ],
                axis=0,
            )
        old = peak[...]
        new = jnp.maximum(old, jnp.max(scores, axis=0, keepdims=True))
        shrink = jnp.exp2(old - new)
        wt = jnp.exp2(scores - new)
        peak[...] = new
        total[...] = total[...] * shrink + jnp.sum(wt, axis=0, keepdims=True)
        wt = wt.astype(BF16)
        accum[0:128, :] = accum[0:128, :] * shrink[:, 0:256] + jnp.dot(
            values[0:128], wt[:, 0:256], preferred_element_type=F32
        )
        accum[128:192, :] = accum[128:192, :] * shrink[:, 256:512] + jnp.dot(
            values[128:192], wt[:, 256:512], preferred_element_type=F32
        )

    def begin(halves, slot):
        keys, vals = project(halves)
        raw = jnp.dot(keys, qt[...], preferred_element_type=F32)
        score[slot] = raw
        value[slot] = vals
        for i in range(4):
            most[slot, i : i + 1, :] = jnp.max(raw[i * HALF : (i + 1) * HALF], axis=0, keepdims=True)

    def finish(blocks, there, slot):
        hidden = [jnp.where((o <= sp) & there, 0.0, NEGATIVE).astype(F32) for o in blocks]
        old = peak[...]
        new = old
        for i in range(4):
            new = jnp.maximum(new, most[slot, i : i + 1, :] * factor + hidden[i])
        shrink = jnp.exp2(old - new)
        peak[...] = new
        parts = [
            jnp.exp2(score[slot, i * HALF : (i + 1) * HALF, :] * factor - (new - hidden[i])) for i in range(4)
        ]
        total[...] = total[...] * shrink + jnp.sum(
            (parts[0] + parts[1]) + (parts[2] + parts[3]), axis=0, keepdims=True
        )
        wt = jnp.concatenate([p.astype(BF16) for p in parts], axis=0)
        accum[0:128, :] = accum[0:128, :] * shrink[:, 0:256] + jnp.dot(
            value[slot, 0:128, :], wt[:, 0:256], preferred_element_type=F32
        )
        accum[128:192, :] = accum[128:192, :] * shrink[:, 256:512] + jnp.dot(
            value[slot, 128:192, :], wt[:, 256:512], preferred_element_type=F32
        )

    score[...] = jnp.zeros_like(score)
    value[...] = jnp.zeros_like(value)
    most[...] = jnp.zeros_like(most)
    peak[...] = jnp.full_like(peak, NEGATIVE)
    total[...] = jnp.zeros_like(total)
    accum[...] = jnp.zeros_like(accum)
    fold([pieces.at[0], pieces.at[1]], None)

    def given(n, count):
        ref = two if count == 2 else lat.at[0, 0]
        remote(ref, ref, p_send.at[0], p_recv.at[n], partner).wait_recv()

    def blocks_of(n):
        kp, km, d = ring_step(n)
        return (
            at(a + rel(kp), b - d), at(a + rel(km), b + d), turned(b + rel(kp), a - d), turned(b + rel(km), a + d)
        )

    def halves_of(o):
        return [lat.at[core, o[0]], lat.at[core, o[1]], lat.at[other, o[2]], lat.at[other, o[3]]]

    def least(o):
        return jnp.minimum(jnp.minimum(o[0], o[1]), jnp.minimum(o[2], o[3]))

    def near_blocks(n):
        return at(a + rel(n), b), turned(b + rel(n), a)

    @pl.loop(0, 3)
    def _(j):
        n = 1 + 2 * j
        latent_near(n)
        latent_near(n + 1)

        @pl.when(j > 0)
        def _():
            given(n - 2, 1)
            given(n - 1, 1)
            one, two_ = near_blocks(n - 2), near_blocks(n - 1)
            o = (one[0], two_[0], one[1], two_[1])

            @pl.when(least(o) <= sp)
            def _():
                begin(halves_of(o), 0)
                finish(o, sp >= 0, 0)

    latent_near(jnp.int32(7))
    latent_far(jnp.int32(8))
    given(jnp.int32(5), 1)
    given(jnp.int32(6), 1)
    one, two_ = near_blocks(jnp.int32(5)), near_blocks(jnp.int32(6))
    last_near = (one[0], two_[0], one[1], two_[1])
    begin(halves_of(last_near), 1)
    latent_far(jnp.int32(9))
    latent_far(jnp.int32(10))
    given(jnp.int32(7), 1)
    seventh = near_blocks(jnp.int32(7))

    @pl.when(jnp.minimum(seventh[0], seventh[1]) <= sp)
    def _():
        fold([lat.at[core, seventh[0]], lat.at[other, seventh[1]]], seventh)

    @pl.loop(0, 14)
    def _(m):
        n = 8 + 2 * m

        @pl.when(n + 3 < 36)
        def _():
            latent_far(n + 3)

        @pl.when(n + 4 < 36)
        def _():
            latent_far(n + 4)

        @pl.when(m == 1)
        def _():
            weights.start()

        @pl.when((m == 4) | (m == 6) | (m == 8))
        def _():
            weights.near(m - 3)
            weights.near(m - 2)

        @pl.when(m == 10)
        def _():
            weights.near(m - 3)
            weights.spread(jnp.int32(0), wown)

            @pl.loop(1, 8)
            def _(k):
                weights.spread(k)

        @pl.when(m == 12)
        def _():
            weights.far(jnp.int32(8))

        @pl.when(m == 13)
        def _():
            weights.far(jnp.int32(9))
            weights.far(jnp.int32(10))

        @pl.when(m == 5)
        def _():
            share_rows()

        @pl.when(m == 9)
        def _():
            share_near()

        now, after = blocks_of(n), blocks_of(n + 1)
        past = blocks_of(n - 1)
        before = [jnp.where(m == 0, o, p) for o, p in zip(last_near, past)]
        given(n, 2)
        given(n + 1, 2)

        @pl.when(jnp.minimum(jnp.minimum(least(before), least(now)), least(after)) <= sp)
        def _():
            begin(halves_of(now), 0)
            finish(before, m >= 0, 1)
            begin(halves_of(after), 1)
            finish(now, m >= 0, 0)

    finish(blocks_of(jnp.int32(35)), sp >= 0, 1)

    result = accum[...]
    att[tp, 0:128, :] = (result[0:128] / total[:, 0:256]).astype(BF16)
    att[tp, 128:192, :] = (result[128:192] / total[:, 256:512]).astype(BF16)

    weights.far(jnp.int32(11))

    for i, dev in enumerate((x_far, x_up, x_dn, partner)):
        remote(att.at[tp], att.at[tp], a_send.at[i], a_recv.at[tp], dev).start()

    share_far()

    @pl.loop(12, 14)
    def _(n):
        weights.far(n)

    for i in (1, 3, 2):
        t = across(i)
        remote(att.at[t], att.at[t], a_send.at[0], a_recv.at[t], partner).wait_recv()
        remote(att.at[t], att.at[t], a_send.at[3 + i], a_recv.at[t], partner).start()
        weights.far(jnp.int32({1: 14, 3: 15, 2: 16}[i]))

    weights.far(jnp.int32(17))

    for i in (0, 1, 2, 3):
        t = 2 * rem(xx + i, 4) + other
        remote(att.at[t], att.at[t], a_send.at[0], a_recv.at[t], partner).wait_recv()
        remote(rows.at[t], rows.at[t], r_send.at[0], r_recv.at[t], partner).wait_recv()
        if i == 2:
            for j, rest in ((10, top), (11, low)):
                remote(wout.at[t, rest], wout.at[t, rest], o_send.at[0], o_recv.at[j], partner).wait_recv()
        else:
            remote(wout.at[t], wout.at[t], o_send.at[0], o_recv.at[t], partner).wait_recv()

    @pl.loop(0, 8)
    def _(t):
        att_t[t] = att[t].T

    @pl.loop(0, 8)
    def _(j):
        cols = pl.ds(pl.multiple_of(j * 256, 256), 256)
        acc = jnp.dot(att_t[0], wout[0, :, cols], preferred_element_type=F32)
        for t in range(1, 8):
            acc = acc + jnp.dot(att_t[t], wout[t, :, cols], preferred_element_type=F32)
        hs[:, cols] = acc
        weights.far(18 + j)

    for i in range(7):
        remote(rows.at[tp], rows.at[tp], r_send.at[i], r_recv.at[tp], partner).wait_send()

    @pl.loop(0, 8)
    def _(t):
        chunk = pl.ds(pl.multiple_of(t * 32, 32), 32)
        value = hs[chunk, :]
        scale = lax.rsqrt(jnp.mean(value * value, axis=-1, keepdims=True) + EPS)
        mixed = (rows[t].astype(F32) + value * scale * again[...]).astype(BF16)
        rows[t] = mixed
        value = mixed.astype(F32)
        scale = lax.rsqrt(jnp.mean(value * value, axis=-1, keepdims=True) + EPS)
        norm[chunk, :] = (value * scale * mgain[...]).astype(BF16)
        weights.far(26 + t)

    weights.far(jnp.int32(34))
    weights.far(jnp.int32(35))

    wts[sp] = wown[...]
    both = jnp.dot(norm[...], wts[:, :, 0:768].reshape(2048, 768), preferred_element_type=F32)
    gate, up = both[:, 0:384], both[:, 384:768]
    hid[...] = (gate / (1.0 + jnp.exp(-gate)) * up).astype(BF16)

    @pl.loop(0, 2)
    def _(j):
        down = wts[pl.ds(j * 32, 32), :, 768:1152].reshape(1024, 384)
        block = lax.dot_general(hid[...], down, (((1,), (1,)), ((), ())), preferred_element_type=F32)
        part[:, :, pl.ds(pl.multiple_of(j * 1024, 1024), 1024)] = block.astype(BF16).reshape(8, 32, 1024)

    for i in (2, 1, 3, 0):
        x_to = rem(xx + i, 4)
        remote(part.at[2 * x_to + other], pbuf.at[x_to], s_send.at[i], s_recv.at[i], partner).start()
    ready = None
    for i, dev in ((2, x_far), (1, x_up), (3, x_dn)):
        x_to = rem(xx + i, 4)
        remote(pbuf.at[x_to], pbuf.at[x_to], s_send.at[i], s_recv.at[i], partner).wait_recv()
        sbuf[i - 1] = (part[2 * x_to + core].astype(F32) + pbuf[x_to].astype(F32)).astype(BF16)
        if ready is not None:
            ready.start()
        ready = remote(sbuf.at[i - 1], rbuf.at[i - 1], s_send.at[3 + i], s_recv.at[3 + i], dev)
    remote(pbuf.at[xx], pbuf.at[xx], s_send.at[0], s_recv.at[0], partner).wait_recv()
    summed = part[tp].astype(F32) + pbuf[xx].astype(F32)
    ready.start()
    @pl.loop(0, 8)
    def _(n):
        for sems in (plus, minus):
            weights.free(sems.at[n])
        given_free(n, 2)

        @pl.when(n != 6)
        def _():
            weights.free(first.at[n])

    for i in (1, 3, 2):
        remote(rbuf.at[i - 1], rbuf.at[i - 1], s_send.at[3 + i], s_recv.at[3 + i], partner).wait_recv()
        summed = summed + rbuf[i - 1].astype(F32)
    out[...] = (rows[tp].astype(F32) + 0.5 * summed).astype(BF16)

    for i in range(7):
        remote(att.at[tp], att.at[tp], a_send.at[i], a_recv.at[tp], partner).wait_send()
        remote(rbuf.at[0], rbuf.at[0], s_send.at[i], s_recv.at[i], partner).wait_send()
    for i in (0, 1, 2, 5, 6):
        remote(wout.at[tp], wout.at[tp], o_send.at[i], o_recv.at[tp], partner).wait_send()
    for i in (3, 4, 7, 8):
        remote(wout.at[tp, top], wout.at[tp, top], o_send.at[i], o_recv.at[tp], partner).wait_send()


def shards(
    residual_in, query_lean, query_broad, latent, rope_key, latent_gain, key_up_lean, key_up_broad, value_up_lean,
    value_up_broad, out_lean, out_broad, attn_gain, mlp_gain, gate_weight, up_weight, down_weight,
):
    tokens = latent.shape[0]
    positions = lax.axis_index("sp") * tokens + jnp.arange(tokens, dtype=jnp.int32)
    freqs = THETA ** (-2.0 * jnp.arange(16, dtype=F32) / 32)
    angle = freqs[:, None] * positions.astype(F32)[None, :]
    vmem = pl.BlockSpec(memory_space=pltpu.VMEM)
    hbm = pl.BlockSpec(memory_space=pl.ANY)
    sems = pltpu.SemaphoreType.DMA
    scratch = [
        pltpu.VMEM((2, PIECE, 256), BF16),
        pltpu.VMEM((2, 512, 512), F32),
        pltpu.VMEM((2, 192, 512), BF16),
        pltpu.VMEM((2, 8, 512), F32),
        pltpu.VMEM((2, 64, PIECE, 256), BF16),
        pltpu.VMEM((64, 32, 1152), BF16),
        pltpu.VMEM((8, 192, 2048), BF16),
        pltpu.VMEM((8, 32, 2048), BF16),
        pltpu.VMEM((8, 192, 256), BF16),
        pltpu.VMEM((256, 512), BF16),
        pltpu.VMEM((256, 256), BF16),
        pltpu.VMEM((192, 256), BF16),
        pltpu.VMEM((32, 256), BF16),
        pltpu.VMEM((1, 512), F32),
        pltpu.VMEM((1, 512), F32),
        pltpu.VMEM((192, 256), F32),
        pltpu.VMEM((8, 256, 192), BF16),
        pltpu.VMEM((256, 2048), F32),
        pltpu.VMEM((256, 2048), BF16),
        pltpu.VMEM((256, 384), BF16),
        pltpu.VMEM((8, 32, 2048), BF16),
        pltpu.VMEM((4, 32, 2048), BF16),
        pltpu.VMEM((3, 32, 2048), BF16),
        pltpu.VMEM((3, 32, 2048), BF16),
        pltpu.VMEM((32, 1152), BF16),
        sems((36,)), sems((36,)), sems((36,)), sems((8,)), sems((8,)), sems((8,)), sems((8,)),
        sems((3,)), sems((9,)), sems((12,)), sems((7,)), sems((8,)), sems((7,)), sems((8,)), sems((7,)), sems((7,)),
    ]
    return pl.pallas_call(
        kernel,
        out_shape=jax.ShapeDtypeStruct((32, 2048), BF16),
        in_specs=[vmem] * 11 + [hbm] * 3 + [vmem] * 5,
        out_specs=vmem,
        scratch_shapes=scratch,
        compiler_params=pltpu.CompilerParams(
            collective_id=0, has_side_effects=True, vmem_limit_bytes=60 * 1024 * 1024
        ),
    )(
        latent, latent_gain[None], rope_key.T, query_broad[:, 0].T, query_lean[:, 0].T, jnp.cos(angle), jnp.sin(angle),
        key_up_broad[:, 0], key_up_lean[:, 0].T, value_up_broad[:, 0], value_up_lean[:, 0].T,
        out_broad[0], out_lean[0], residual_in, attn_gain[None], mlp_gain[None], gate_weight, up_weight, down_weight.T,
    )


def solution(mesh):
    in_specs = (
        P(("sp", "tp"), None), P("sp", "tp", None), P("sp", "tp", None), P("sp", None), P("sp", None), P(),
        P(None, "tp", None), P(None, "tp", None), P(None, "tp", None), P(None, "tp", None),
        P("tp", None, None), P("tp", None, None), P(), P(), P("sp", "tp"), P("sp", "tp"), P("tp", "sp"),
    )
    return jax.shard_map(
        shards, mesh=mesh, in_specs=in_specs, out_specs=P(("sp", "tp"), None), check_vma=False
    )
```

time: 125 us -> 94.8 us (0.76)
  Pallas kernels: 114 us -> 92.3 us
  local copies, waits for them, and re-layouts: 6.99 us -> 1.57 us
  other arithmetic: 2.91 us -> 0.77 us
    pallas_call x1, Pallas kernels: 114 us -> 92.3 us  [shards(): pl.pallas_call(kernel, out_shape=jax.ShapeDtypeStruct((32, 2048), BF16),...]
    unnamed x21 -> x1, local copies, waits for them, and re-layouts: 6.43 us -> 1.57 us
    concatenate x3 -> x0, other arithmetic: 1.38 us -> none  [the longest x1 0.72 us: shards(): jnp.concatenate([jnp.concatenate([broad[:, :128], pad((tokens, 64)), roun...]
where the time goes in v2:
time: 94.8 us; the launch traced here: 94.7 us
  Pallas kernels  92.3 us (97%)
  local copies, waits for them, and re-layouts  1.57 us (2%)
    pallas_call x1, Pallas kernels, shards(): pl.pallas_call(kernel, out_shape=jax.ShapeDtypeStruct((32, 2048), BF16),...  92.3 us

profile of v2, /device:TPU:1, one launch (start us, length us, event | category | flops | bytes accessed | tf_op | source)
XLA Modules:
  0.0 94.7 jit_solution(7261297880681421353)
XLA Ops:
  0.0 0.8 multiply_sine_fusion
  0.8 92.3 %shard_map.163 = bf16[32,2048]{1,0:T(8,128)(2,1)} custom-call(bf16[256,256]{1,0:T(8,128)(2,1)} %latent.1, f32[1,256]{1,0:T(1,128)} %bitcast.33, bf16[32,256]{1,0:T(8,128)(2,1)} %bitcast.30, bf16[160,256]{1,0:T(8,128)(2,1)} %bitcast.23, bf16[96,256]{1,0:T(8,128)(2,1)} %bitcast.26, f32[16,256]{1,0:T(8,128)} %get-tuple-element.6.cosine, ...), custom_call_target="tpu_custom_call" | custom-call | tf_op jit(solution)/shard_map/pallas_call | solution.py:601
  93.1 1.6 %copy.19 = bf16[32,2048]{1,0:T(8,128)(2,1)} copy(bf16[32,2048]{1,0:T(8,128)(2,1)} %shard_map.163) | data formatting | bytes 262144
  (2 shorter events, 0.0 us)

commit v3 on v2

--- a/solution.py
+++ b/solution.py
@@ -27,9 +27,16 @@
 
 
 def kernel(
-    latent, lgain, rope, qb, ql, cosine, sine, kb, kl, vb, vl, ob, ol, resid, again, mgain, gate_w, up_w, down_w,
-    out,
-    pieces, score, value, most, lat, wts, wout, rows, att, qt, kup, vupt, spread, peak, total, accum, att_t, hs, norm, hid, part, pbuf, sbuf, rbuf, wown,
+    *args,
+):
+    inputs, (ob, ol, resid, out), rest = args[:16], args[16:20], args[20:]
+    held, rest, in_sem = rest[:16], rest[16:-1], rest[-1]
+    run(inputs, held, in_sem, ob, ol, resid, out, *rest)
+
+
+def run(
+    inputs, held, in_sem, ob, ol, resid, out,
+    pieces, score, value, most, lat, wts, wout, rows, att, qt, kup, vupt, spread, peak, total, accum, att_t, hs, norm, hid, part, pbuf, sbuf, rbuf, cbuf, wown,
     l_recv, w_recv, p_recv, first, plus, minus, p_send,
     loc, o_send, o_recv, r_send, r_recv, a_send, a_recv, s_send, s_recv,
 ):
@@ -55,6 +62,7 @@
     a_up, a_dn, b_up, b_dn = (
         (at(a + 1, b), tp), (at(a - 1, b), tp), (at(a, b + 1), tp), (at(a, b - 1), tp)
     )
+    a_up2, a_dn2 = (at(a + 2, b), tp), (at(a - 2, b), tp)
     partner = (sp, 2 * xx + other)
 
     def across(step):
@@ -66,6 +74,14 @@
         return pltpu.make_async_remote_copy(
             src_ref=src, dst_ref=dst, send_sem=ssem, recv_sem=rsem, device_id=dev, device_id_type=MESH
         )
+
+    latent, lgain, rope, cosine, sine, qb, ql, kb, kl, vb, vl, again, mgain, gate_w, up_w, down_w = held
+    barrier = pltpu.get_barrier_semaphore()
+    for dev in (a_up, a_dn, b_up, b_dn, partner, x_up, x_far, x_dn, a_up2, a_dn2):
+        pl.semaphore_signal(barrier, inc=1, device_id=dev, device_id_type=MESH)
+    loads = [pltpu.make_async_copy(src, dst, in_sem.at[i]) for i, (src, dst) in enumerate(zip(inputs, held))]
+    for load in loads:
+        load.start()
 
     own_b = pltpu.make_async_copy(ob, wout.at[tp, pl.ds(0, 128)], loc.at[0])
     own_l = pltpu.make_async_copy(ol, wout.at[tp, pl.ds(128, 64)], loc.at[1])
@@ -74,9 +90,8 @@
     own_l.start()
     own_r.start()
 
-    barrier = pltpu.get_barrier_semaphore()
-    for dev in (a_up, a_dn, b_up, b_dn, partner, x_up, x_far, x_dn):
-        pl.semaphore_signal(barrier, inc=1, device_id=dev, device_id_type=MESH)
+    for load in loads[:7]:
+        load.wait()
 
     def rotated(ref, start):
         low, high = ref[start : start + 16, :].astype(F32), ref[start + 16 : start + 32, :].astype(F32)
@@ -90,7 +105,8 @@
         pieces[h, 0:HALF, :] = wide[h * HALF : (h + 1) * HALF]
         pieces[h, HALF:PIECE, 0:HALF] = low[:, h * HALF : (h + 1) * HALF]
         pieces[h, HALF:PIECE, HALF:256] = high[:, h * HALF : (h + 1) * HALF]
-    qt[...] = jnp.zeros_like(qt)
+    qt[128:256, :] = jnp.zeros((128, 512), BF16)
+    qt[0:128, 256:512] = jnp.zeros((128, 256), BF16)
     qt[0:128, 0:256] = qb[0:128, :]
     qt[128:192, 256:512] = ql[0:64, :]
     for ref, start, at_column in ((qb, 128, 0), (ql, 64, 256)):
@@ -98,7 +114,9 @@
         qt[192:208, at_column : at_column + 256] = low
         qt[208:224, at_column : at_column + 256] = high
 
-    pl.semaphore_wait(barrier, 8)
+    for load in loads[7:]:
+        load.wait()
+    pl.semaphore_wait(barrier, 10)
 
     class Stream:
         def __init__(self, own, slot, pair, recv, fresh):
@@ -179,9 +197,18 @@
     weights = Stream(wown, lambda o: wts.at[o], wts.at[pl.ds(0, 2)], w_recv, False)
 
     def latent_near(k):
-        latents.near(k)
-        latents.spread(k)
-        give(k, at(a + rel(k), b))
+        o = at(a + rel(k), b)
+        remote(lat.at[core, o], lat.at[core, o], first.at[0], l_recv.at[k], partner).wait_recv()
+
+        @pl.when((k == 1) | (k == 3))
+        def _():
+            latents.go(lat.at[core, o], o, first.at[k], k + 4, a_up2)
+
+        @pl.when(k == 2)
+        def _():
+            latents.go(lat.at[core, o], o, first.at[k], k + 4, a_dn2)
+
+        give(k, o)
 
     def latent_far(n):
         k, op, om = latents.far(n)
@@ -198,7 +225,8 @@
         give(n, om)
 
     latents.start()
-    latents.spread(jnp.int32(0), pieces.at[core])
+    latents.go(latents.own, sp, first.at[5], 3, a_up2)
+    latents.go(latents.own, sp, first.at[4], 4, a_dn2)
 
     own_r.wait()
     for i, dev in enumerate((partner, x_up, x_dn, x_far)):
@@ -237,10 +265,6 @@
     spread[...] = (
         lax.broadcasted_iota(jnp.int32, (32, 256), 1) == lax.broadcasted_iota(jnp.int32, (32, 256), 0) + 192
     ).astype(F32).astype(BF16)
-    wown[...] = jnp.zeros_like(wown)
-    wown[:, 0:352] = gate_w[...]
-    wown[:, 384:736] = up_w[...]
-    wown[:, 768:1120] = down_w[...]
 
     column = lax.broadcasted_iota(jnp.int32, (1, 512), 1)
     factor = jnp.where(column < 256, LOG2E * 160 ** (-0.5), LOG2E * 96 ** (-0.5)).astype(F32)
@@ -322,9 +346,6 @@
             value[slot, 128:192, :], wt[:, 256:512], preferred_element_type=F32
         )
 
-    score[...] = jnp.zeros_like(score)
-    value[...] = jnp.zeros_like(value)
-    most[...] = jnp.zeros_like(most)
     peak[...] = jnp.full_like(peak, NEGATIVE)
     total[...] = jnp.zeros_like(total)
     accum[...] = jnp.zeros_like(accum)
@@ -349,33 +370,44 @@
     def near_blocks(n):
         return at(a + rel(n), b), turned(b + rel(n), a)
 
-    @pl.loop(0, 3)
-    def _(j):
-        n = 1 + 2 * j
-        latent_near(n)
-        latent_near(n + 1)
-
-        @pl.when(j > 0)
-        def _():
-            given(n - 2, 1)
-            given(n - 1, 1)
-            one, two_ = near_blocks(n - 2), near_blocks(n - 1)
-            o = (one[0], two_[0], one[1], two_[1])
-
-            @pl.when(least(o) <= sp)
-            def _():
-                begin(halves_of(o), 0)
-                finish(o, sp >= 0, 0)
-
-    latent_near(jnp.int32(7))
+    latents.spread(jnp.int32(0), pieces.at[core])
+
+    def near_pair(n, slot):
+        given(n, 1)
+        given(n + 1, 1)
+        one, two_ = near_blocks(n), near_blocks(n + 1)
+        o = (one[0], two_[0], one[1], two_[1])
+        begin(halves_of(o), slot)
+        return o
+
+    one_, two__, three, four, five, six, seven = (jnp.int32(i) for i in range(1, 8))
+    latent_near(one_)
+    latent_near(two__)
+    latent_near(three)
+    latent_near(four)
+    latents.spread(one_)
+    latents.spread(two__)
+    wown[...] = jnp.zeros_like(wown)
+    wown[:, 0:352] = gate_w[...]
+    wown[:, 384:736] = up_w[...]
+    wown[:, 768:1120] = down_w[...]
+    score[...] = jnp.zeros_like(score)
+    value[...] = jnp.zeros_like(value)
+    most[...] = jnp.zeros_like(most)
+    finish(near_pair(one_, 0), sp >= 0, 0)
+    latents.spread(three)
+    latents.spread(four)
     latent_far(jnp.int32(8))
-    given(jnp.int32(5), 1)
-    given(jnp.int32(6), 1)
-    one, two_ = near_blocks(jnp.int32(5)), near_blocks(jnp.int32(6))
-    last_near = (one[0], two_[0], one[1], two_[1])
-    begin(halves_of(last_near), 1)
+    finish(near_pair(three, 0), sp >= 0, 0)
+    latent_near(five)
+    latent_near(six)
+    latent_near(seven)
+    latents.spread(five)
+    latents.spread(six)
+    latents.spread(seven)
     latent_far(jnp.int32(9))
     latent_far(jnp.int32(10))
+    last_near = near_pair(five, 1)
     given(jnp.int32(7), 1)
     seventh = near_blocks(jnp.int32(7))
 
@@ -451,26 +483,45 @@
 
     weights.far(jnp.int32(11))
 
-    for i, dev in enumerate((x_far, x_up, x_dn, partner)):
-        remote(att.at[tp], att.at[tp], a_send.at[i], a_recv.at[tp], dev).start()
+    def att_copy(t, half, i, dev):
+        ref = att.at[t] if half is None else att.at[t, half]
+        return remote(ref, ref, a_send.at[i], a_recv.at[i], dev)
+
+    for half, i, dev in ((top, 0, x_up), (low, 2, x_dn), (low, 1, x_up), (top, 3, x_dn), (None, 6, partner)):
+        att_copy(tp, half, i, dev).start()
 
     share_far()
 
-    @pl.loop(12, 14)
+    @pl.loop(12, 15)
     def _(n):
         weights.far(n)
 
-    for i in (1, 3, 2):
-        t = across(i)
-        remote(att.at[t], att.at[t], a_send.at[0], a_recv.at[t], partner).wait_recv()
-        remote(att.at[t], att.at[t], a_send.at[3 + i], a_recv.at[t], partner).start()
-        weights.far(jnp.int32({1: 14, 3: 15, 2: 16}[i]))
-
-    weights.far(jnp.int32(17))
+    t_up, t_dn, t_far = across(3), across(1), across(2)
+    att_copy(t_up, top, 0, partner).wait_recv()
+    att_copy(t_up, top, 4, x_up).start()
+    att_copy(t_dn, low, 2, partner).wait_recv()
+    att_copy(t_dn, low, 5, x_dn).start()
+    weights.far(jnp.int32(15))
+    att_copy(t_up, low, 1, partner).wait_recv()
+    att_copy(t_up, None, 8, partner).start()
+    att_copy(t_dn, top, 3, partner).wait_recv()
+    att_copy(t_dn, None, 7, partner).start()
+
+    @pl.loop(16, 18)
+    def _(n):
+        weights.far(n)
+
+    att_copy(t_far, top, 4, partner).wait_recv()
+    att_copy(t_far, top, 9, partner).start()
+    att_copy(t_far, low, 5, partner).wait_recv()
+    att_copy(t_far, low, 10, partner).start()
+    weights.far(jnp.int32(18))
+
+    for half, i in ((None, 6), (None, 7), (None, 8), (top, 9), (low, 10)):
+        att_copy(tp, half, i, partner).wait_recv()
 
     for i in (0, 1, 2, 3):
         t = 2 * rem(xx + i, 4) + other
-        remote(att.at[t], att.at[t], a_send.at[0], a_recv.at[t], partner).wait_recv()
         remote(rows.at[t], rows.at[t], r_send.at[0], r_recv.at[t], partner).wait_recv()
         if i == 2:
             for j, rest in ((10, top), (11, low)):
@@ -482,14 +533,15 @@
     def _(t):
         att_t[t] = att[t].T
 
-    @pl.loop(0, 8)
+    @pl.loop(0, 4)
     def _(j):
-        cols = pl.ds(pl.multiple_of(j * 256, 256), 256)
+        cols = pl.ds(pl.multiple_of(j * 512, 512), 512)
         acc = jnp.dot(att_t[0], wout[0, :, cols], preferred_element_type=F32)
         for t in range(1, 8):
             acc = acc + jnp.dot(att_t[t], wout[t, :, cols], preferred_element_type=F32)
         hs[:, cols] = acc
-        weights.far(18 + j)
+        weights.far(19 + 2 * j)
+        weights.far(20 + 2 * j)
 
     for i in range(7):
         remote(rows.at[tp], rows.at[tp], r_send.at[i], r_recv.at[tp], partner).wait_send()
@@ -504,9 +556,8 @@
         value = mixed.astype(F32)
         scale = lax.rsqrt(jnp.mean(value * value, axis=-1, keepdims=True) + EPS)
         norm[chunk, :] = (value * scale * mgain[...]).astype(BF16)
-        weights.far(26 + t)
-
-    weights.far(jnp.int32(34))
+        weights.far(27 + t)
+
     weights.far(jnp.int32(35))
 
     wts[sp] = wown[...]
@@ -523,17 +574,28 @@
     for i in (2, 1, 3, 0):
         x_to = rem(xx + i, 4)
         remote(part.at[2 * x_to + other], pbuf.at[x_to], s_send.at[i], s_recv.at[i], partner).start()
-    ready = None
-    for i, dev in ((2, x_far), (1, x_up), (3, x_dn)):
+    def chip_sum(i):
         x_to = rem(xx + i, 4)
         remote(pbuf.at[x_to], pbuf.at[x_to], s_send.at[i], s_recv.at[i], partner).wait_recv()
-        sbuf[i - 1] = (part[2 * x_to + core].astype(F32) + pbuf[x_to].astype(F32)).astype(BF16)
-        if ready is not None:
-            ready.start()
-        ready = remote(sbuf.at[i - 1], rbuf.at[i - 1], s_send.at[3 + i], s_recv.at[3 + i], dev)
-    remote(pbuf.at[xx], pbuf.at[xx], s_send.at[0], s_recv.at[0], partner).wait_recv()
-    summed = part[tp].astype(F32) + pbuf[xx].astype(F32)
-    ready.start()
+        return part[2 * x_to + core].astype(F32) + pbuf[x_to].astype(F32)
+
+    upper, under = pl.ds(0, 16), pl.ds(16, 16)
+
+    def along(src, dst, i, dev):
+        return remote(src, dst, s_send.at[i], s_recv.at[i], dev)
+
+    far_sum = chip_sum(2)
+    sbuf[1] = far_sum.astype(BF16)
+    up_sum = chip_sum(1)
+    sbuf[0] = up_sum.astype(BF16)
+    along(sbuf.at[1, upper], rbuf.at[1, upper], 4, x_up).start()
+    along(sbuf.at[1, under], rbuf.at[1, under], 5, x_dn).start()
+    dn_sum = chip_sum(3)
+    sbuf[2] = dn_sum.astype(BF16)
+    along(sbuf.at[0, under], rbuf.at[0, under], 6, x_up).start()
+    summed = chip_sum(0)
+    along(sbuf.at[2, upper], rbuf.at[2, upper], 7, x_dn).start()
+
     @pl.loop(0, 8)
     def _(n):
         for sems in (plus, minus):
@@ -544,18 +606,36 @@
         def _():
             weights.free(first.at[n])
 
-    for i in (1, 3, 2):
-        remote(rbuf.at[i - 1], rbuf.at[i - 1], s_send.at[3 + i], s_recv.at[3 + i], partner).wait_recv()
-        summed = summed + rbuf[i - 1].astype(F32)
-    out[...] = (rows[tp].astype(F32) + 0.5 * summed).astype(BF16)
-
-    for i in range(7):
-        remote(att.at[tp], att.at[tp], a_send.at[i], a_recv.at[tp], partner).wait_send()
-        remote(rbuf.at[0], rbuf.at[0], s_send.at[i], s_recv.at[i], partner).wait_send()
+    for i in range(11):
+        half = (top, low, low, top, top, low, None, None, None, top, low)[i]
+        att_copy(tp, half, i, partner).wait_send()
     for i in (0, 1, 2, 5, 6):
         remote(wout.at[tp], wout.at[tp], o_send.at[i], o_recv.at[tp], partner).wait_send()
     for i in (3, 4, 7, 8):
         remote(wout.at[tp, top], wout.at[tp, top], o_send.at[i], o_recv.at[tp], partner).wait_send()
+
+    along(rbuf.at[1, upper], rbuf.at[1, upper], 4, partner).wait_recv()
+    cbuf[0] = (sums_of(part, pbuf, rem(xx + 1, 4), core, 0) + rbuf[1, 0:16].astype(F32)).astype(BF16)
+    along(rbuf.at[1, under], rbuf.at[1, under], 5, partner).wait_recv()
+    cbuf[1] = (sums_of(part, pbuf, rem(xx + 3, 4), core, 16) + rbuf[1, 16:32].astype(F32)).astype(BF16)
+    along(cbuf.at[0], rbuf.at[0, upper], 8, x_up).start()
+    along(cbuf.at[1], rbuf.at[2, under], 9, x_dn).start()
+    along(rbuf.at[0, under], rbuf.at[0, under], 6, partner).wait_recv()
+    along(rbuf.at[2, upper], rbuf.at[2, upper], 7, partner).wait_recv()
+    along(rbuf.at[0, upper], rbuf.at[0, upper], 8, partner).wait_recv()
+    along(rbuf.at[2, under], rbuf.at[2, under], 9, partner).wait_recv()
+    summed = summed + (rbuf[0].astype(F32) + rbuf[2].astype(F32))
+    out[...] = (rows[tp].astype(F32) + 0.5 * summed).astype(BF16)
+
+    for i in range(4):
+        remote(rbuf.at[0], rbuf.at[0], s_send.at[i], s_recv.at[i], partner).wait_send()
+    for i in range(4, 10):
+        along(rbuf.at[0, upper], rbuf.at[0, upper], i, partner).wait_send()
+
+
+def sums_of(part, pbuf, x_to, core, start):
+    rows = slice(start, start + 16)
+    return part[2 * x_to + core, rows].astype(F32) + pbuf[x_to, rows].astype(F32)
 
 
 def shards(
@@ -569,7 +649,12 @@
     vmem = pl.BlockSpec(memory_space=pltpu.VMEM)
     hbm = pl.BlockSpec(memory_space=pl.ANY)
     sems = pltpu.SemaphoreType.DMA
-    scratch = [
+    loaded = [
+        ((256, 256), BF16), ((1, 256), F32), ((32, 256), BF16), ((16, 256), F32), ((16, 256), F32), ((160, 256), BF16),
+        ((96, 256), BF16), ((256, 128), BF16), ((64, 256), BF16), ((256, 128), BF16), ((64, 256), BF16),
+        ((1, 2048), F32), ((1, 2048), F32), ((32, 352), BF16), ((32, 352), BF16), ((32, 352), BF16),
+    ]
+    scratch = [pltpu.VMEM(shape, dtype) for shape, dtype in loaded] + [
         pltpu.VMEM((2, PIECE, 256), BF16),
         pltpu.VMEM((2, 512, 512), F32),
         pltpu.VMEM((2, 192, 512), BF16),
@@ -594,23 +679,33 @@
         pltpu.VMEM((4, 32, 2048), BF16),
         pltpu.VMEM((3, 32, 2048), BF16),
         pltpu.VMEM((3, 32, 2048), BF16),
+        pltpu.VMEM((2, 16, 2048), BF16),
         pltpu.VMEM((32, 1152), BF16),
         sems((36,)), sems((36,)), sems((36,)), sems((8,)), sems((8,)), sems((8,)), sems((8,)),
-        sems((3,)), sems((9,)), sems((12,)), sems((7,)), sems((8,)), sems((7,)), sems((8,)), sems((7,)), sems((7,)),
+        sems((3,)), sems((9,)), sems((12,)), sems((7,)), sems((8,)), sems((11,)), sems((11,)), sems((10,)), sems((10,)),
+        sems((16,)),
     ]
     return pl.pallas_call(
         kernel,
         out_shape=jax.ShapeDtypeStruct((32, 2048), BF16),
-        in_specs=[vmem] * 11 + [hbm] * 3 + [vmem] * 5,
+        in_specs=[hbm] * 19,
         out_specs=vmem,
         scratch_shapes=scratch,
         compiler_params=pltpu.CompilerParams(
-            collective_id=0, has_side_effects=True, vmem_limit_bytes=60 * 1024 * 1024
+            collective_id=0, has_side_effects=True, vmem_limit_bytes=44 * 1024 * 1024
         ),
     )(
-        latent, latent_gain[None], rope_key.T, query_broad[:, 0].T, query_lean[:, 0].T, jnp.cos(angle), jnp.sin(angle),
-        key_up_broad[:, 0], key_up_lean[:, 0].T, value_up_broad[:, 0], value_up_lean[:, 0].T,
-        out_broad[0], out_lean[0], residual_in, attn_gain[None], mlp_gain[None], gate_weight, up_weight, down_weight.T,
+        *[pltpu.with_memory_space_constraint(v, pltpu.HBM) for v in (latent, latent_gain[None], rope_key.T)],
+        jnp.cos(angle),
+        jnp.sin(angle),
+        *[
+            pltpu.with_memory_space_constraint(v, pltpu.HBM)
+            for v in (
+                query_broad[:, 0].T, query_lean[:, 0].T, key_up_broad[:, 0], key_up_lean[:, 0].T, value_up_broad[:, 0],
+                value_up_lean[:, 0].T, attn_gain[None], mlp_gain[None], gate_weight, up_weight, down_weight.T,
+                out_broad[0], out_lean[0], residual_in,
+            )
+        ],
     )
 
 

time: 94.8 us -> 88.4 us (0.932)
  Pallas kernels: 92.3 us -> 87.5 us
    pallas_call x1, Pallas kernels: 92.3 us -> 87.5 us  [shards(): pl.pallas_call(kernel, out_shape=jax.ShapeDtypeStruct((32, 2048), BF16),...]
where the time goes in v3:
time: 88.4 us; the launch traced here: 88.3 us
  Pallas kernels  87.5 us (99%)
    pallas_call x1, Pallas kernels, shards(): pl.pallas_call(kernel, out_shape=jax.ShapeDtypeStruct((32, 2048), BF16),...  87.5 us

profile of v3, /device:TPU:1, one launch (start us, length us, event | category | flops | bytes accessed | tf_op | source)
XLA Modules:
  0.0 88.3 jit_solution(3359267078926237591)
XLA Ops:
  0.0 0.1 multiply_sine_fusion
  0.2 87.5 %shard_map.163 = bf16[32,2048]{1,0:T(8,128)(2,1)S(1)} custom-call(bf16[256,256]{1,0:T(8,128)(2,1)} %args_0_.4, f32[1,256]{1,0:T(1,128)} %bitcast.33, bf16[32,256]{1,0:T(8,128)(2,1)} %bitcast.30, f32[16,256]{1,0:T(8,128)S(1)} %get-tuple-element.6.args_3_, f32[16,256]{1,0:T(8,128)S(1)} %get-tuple-element.5.args_4_, bf16[160,256]{1,0:T(8,128)(2,1)} %bitcast.23, ...), custom_call_target="tpu_custom_call" | custom-call | tf_op jit(solution)/shard_map/pallas_call | solution.py:688
  87.6 0.7 copy.19
  (2 shorter events, 0.0 us)

commit v4 on v3

--- a/solution.py
+++ b/solution.py
@@ -481,7 +481,7 @@
     att[tp, 0:128, :] = (result[0:128] / total[:, 0:256]).astype(BF16)
     att[tp, 128:192, :] = (result[128:192] / total[:, 256:512]).astype(BF16)
 
-    weights.far(jnp.int32(11))
+    share_far()
 
     def att_copy(t, half, i, dev):
         ref = att.at[t] if half is None else att.at[t, half]
@@ -490,9 +490,7 @@
     for half, i, dev in ((top, 0, x_up), (low, 2, x_dn), (low, 1, x_up), (top, 3, x_dn), (None, 6, partner)):
         att_copy(tp, half, i, dev).start()
 
-    share_far()
-
-    @pl.loop(12, 15)
+    @pl.loop(11, 17)
     def _(n):
         weights.far(n)
 
@@ -501,13 +499,14 @@
     att_copy(t_up, top, 4, x_up).start()
     att_copy(t_dn, low, 2, partner).wait_recv()
     att_copy(t_dn, low, 5, x_dn).start()
-    weights.far(jnp.int32(15))
+    weights.far(jnp.int32(17))
+    weights.far(jnp.int32(18))
     att_copy(t_up, low, 1, partner).wait_recv()
     att_copy(t_up, None, 8, partner).start()
     att_copy(t_dn, top, 3, partner).wait_recv()
     att_copy(t_dn, None, 7, partner).start()
 
-    @pl.loop(16, 18)
+    @pl.loop(19, 21)
     def _(n):
         weights.far(n)
 
@@ -515,7 +514,8 @@
     att_copy(t_far, top, 9, partner).start()
     att_copy(t_far, low, 5, partner).wait_recv()
     att_copy(t_far, low, 10, partner).start()
-    weights.far(jnp.int32(18))
+    weights.far(jnp.int32(21))
+    weights.far(jnp.int32(22))
 
     for half, i in ((None, 6), (None, 7), (None, 8), (top, 9), (low, 10)):
         att_copy(tp, half, i, partner).wait_recv()
@@ -540,8 +540,8 @@
         for t in range(1, 8):
             acc = acc + jnp.dot(att_t[t], wout[t, :, cols], preferred_element_type=F32)
         hs[:, cols] = acc
-        weights.far(19 + 2 * j)
-        weights.far(20 + 2 * j)
+        weights.far(23 + 2 * j)
+        weights.far(24 + 2 * j)
 
     for i in range(7):
         remote(rows.at[tp], rows.at[tp], r_send.at[i], r_recv.at[tp], partner).wait_send()
@@ -556,45 +556,56 @@
         value = mixed.astype(F32)
         scale = lax.rsqrt(jnp.mean(value * value, axis=-1, keepdims=True) + EPS)
         norm[chunk, :] = (value * scale * mgain[...]).astype(BF16)
-        weights.far(27 + t)
-
-    weights.far(jnp.int32(35))
+
+        @pl.when(t < 5)
+        def _():
+            weights.far(31 + t)
+
 
     wts[sp] = wown[...]
     both = jnp.dot(norm[...], wts[:, :, 0:768].reshape(2048, 768), preferred_element_type=F32)
     gate, up = both[:, 0:384], both[:, 384:768]
     hid[...] = (gate / (1.0 + jnp.exp(-gate)) * up).astype(BF16)
 
-    @pl.loop(0, 2)
-    def _(j):
-        down = wts[pl.ds(j * 32, 32), :, 768:1152].reshape(1024, 384)
+    upper, under = pl.ds(0, 16), pl.ds(16, 16)
+    sides = (pl.ds(0, 1024), pl.ds(1024, 1024))
+
+    def chip_copy(i, q):
+        x_to = rem(xx + i, 4)
+        return remote(
+            part.at[2 * x_to + other, :, sides[q]], pbuf.at[x_to, :, sides[q]], s_send.at[10 * q + i],
+            s_recv.at[10 * q + i], partner,
+        )
+
+    def chip_sum(i, q):
+        chip_copy(i, q).wait_recv()
+        return both_of(i, q, slice(0, 32))
+
+    def both_of(i, q, picked):
+        x_to = rem(xx + i, 4)
+        return part[2 * x_to + core, picked, sides[q]].astype(F32) + pbuf[x_to, picked, sides[q]].astype(F32)
+
+    def along(src, dst, i, q, dev):
+        return remote(src, dst, s_send.at[10 * q + i], s_recv.at[10 * q + i], dev)
+
+    for q in range(2):
+        down = wts[32 * q : 32 * q + 32, :, 768:1152].reshape(1024, 384)
         block = lax.dot_general(hid[...], down, (((1,), (1,)), ((), ())), preferred_element_type=F32)
-        part[:, :, pl.ds(pl.multiple_of(j * 1024, 1024), 1024)] = block.astype(BF16).reshape(8, 32, 1024)
-
-    for i in (2, 1, 3, 0):
-        x_to = rem(xx + i, 4)
-        remote(part.at[2 * x_to + other], pbuf.at[x_to], s_send.at[i], s_recv.at[i], partner).start()
-    def chip_sum(i):
-        x_to = rem(xx + i, 4)
-        remote(pbuf.at[x_to], pbuf.at[x_to], s_send.at[i], s_recv.at[i], partner).wait_recv()
-        return part[2 * x_to + core].astype(F32) + pbuf[x_to].astype(F32)
-
-    upper, under = pl.ds(0, 16), pl.ds(16, 16)
-
-    def along(src, dst, i, dev):
-        return remote(src, dst, s_send.at[i], s_recv.at[i], dev)
-
-    far_sum = chip_sum(2)
-    sbuf[1] = far_sum.astype(BF16)
-    up_sum = chip_sum(1)
-    sbuf[0] = up_sum.astype(BF16)
-    along(sbuf.at[1, upper], rbuf.at[1, upper], 4, x_up).start()
-    along(sbuf.at[1, under], rbuf.at[1, under], 5, x_dn).start()
-    dn_sum = chip_sum(3)
-    sbuf[2] = dn_sum.astype(BF16)
-    along(sbuf.at[0, under], rbuf.at[0, under], 6, x_up).start()
-    summed = chip_sum(0)
-    along(sbuf.at[2, upper], rbuf.at[2, upper], 7, x_dn).start()
+        part[:, :, sides[q]] = block.astype(BF16).reshape(8, 32, 1024)
+        for i in (2, 1, 3, 0):
+            chip_copy(i, q).start()
+
+    summed = []
+    for q in range(2):
+        side = sides[q]
+        sbuf[1, :, side] = chip_sum(2, q).astype(BF16)
+        sbuf[0, :, side] = chip_sum(1, q).astype(BF16)
+        along(sbuf.at[1, upper, side], rbuf.at[1, upper, side], 4, q, x_up).start()
+        along(sbuf.at[1, under, side], rbuf.at[1, under, side], 5, q, x_dn).start()
+        sbuf[2, :, side] = chip_sum(3, q).astype(BF16)
+        along(sbuf.at[0, under, side], rbuf.at[0, under, side], 6, q, x_up).start()
+        summed.append(chip_sum(0, q))
+        along(sbuf.at[2, upper, side], rbuf.at[2, upper, side], 7, q, x_dn).start()
 
     @pl.loop(0, 8)
     def _(n):
@@ -614,28 +625,26 @@
     for i in (3, 4, 7, 8):
         remote(wout.at[tp, top], wout.at[tp, top], o_send.at[i], o_recv.at[tp], partner).wait_send()
 
-    along(rbuf.at[1, upper], rbuf.at[1, upper], 4, partner).wait_recv()
-    cbuf[0] = (sums_of(part, pbuf, rem(xx + 1, 4), core, 0) + rbuf[1, 0:16].astype(F32)).astype(BF16)
-    along(rbuf.at[1, under], rbuf.at[1, under], 5, partner).wait_recv()
-    cbuf[1] = (sums_of(part, pbuf, rem(xx + 3, 4), core, 16) + rbuf[1, 16:32].astype(F32)).astype(BF16)
-    along(cbuf.at[0], rbuf.at[0, upper], 8, x_up).start()
-    along(cbuf.at[1], rbuf.at[2, under], 9, x_dn).start()
-    along(rbuf.at[0, under], rbuf.at[0, under], 6, partner).wait_recv()
-    along(rbuf.at[2, upper], rbuf.at[2, upper], 7, partner).wait_recv()
-    along(rbuf.at[0, upper], rbuf.at[0, upper], 8, partner).wait_recv()
-    along(rbuf.at[2, under], rbuf.at[2, under], 9, partner).wait_recv()
-    summed = summed + (rbuf[0].astype(F32) + rbuf[2].astype(F32))
-    out[...] = (rows[tp].astype(F32) + 0.5 * summed).astype(BF16)
-
-    for i in range(4):
-        remote(rbuf.at[0], rbuf.at[0], s_send.at[i], s_recv.at[i], partner).wait_send()
-    for i in range(4, 10):
-        along(rbuf.at[0, upper], rbuf.at[0, upper], i, partner).wait_send()
-
-
-def sums_of(part, pbuf, x_to, core, start):
-    rows = slice(start, start + 16)
-    return part[2 * x_to + core, rows].astype(F32) + pbuf[x_to, rows].astype(F32)
+    for q in range(2):
+        side = sides[q]
+        along(rbuf.at[1, upper, side], rbuf.at[1, upper, side], 4, q, partner).wait_recv()
+        cbuf[0, :, side] = (both_of(1, q, slice(0, 16)) + rbuf[1, 0:16, side].astype(F32)).astype(BF16)
+        along(rbuf.at[1, under, side], rbuf.at[1, under, side], 5, q, partner).wait_recv()
+        cbuf[1, :, side] = (both_of(3, q, slice(16, 32)) + rbuf[1, 16:32, side].astype(F32)).astype(BF16)
+        along(cbuf.at[0, :, side], rbuf.at[0, upper, side], 8, q, x_up).start()
+        along(cbuf.at[1, :, side], rbuf.at[2, under, side], 9, q, x_dn).start()
+    for q in range(2):
+        side = sides[q]
+        for i, r, picked in ((6, 0, under), (7, 2, upper), (8, 0, upper), (9, 2, under)):
+            along(rbuf.at[r, picked, side], rbuf.at[r, picked, side], i, q, partner).wait_recv()
+        value_q = summed[q] + (rbuf[0, :, side].astype(F32) + rbuf[2, :, side].astype(F32))
+        out[:, side] = (rows[tp, :, side].astype(F32) + 0.5 * value_q).astype(BF16)
+
+    for q in range(2):
+        for i in range(4):
+            chip_copy(i, q).wait_send()
+        for i in range(4, 10):
+            along(rbuf.at[0, upper, sides[q]], rbuf.at[0, upper, sides[q]], i, q, partner).wait_send()
 
 
 def shards(
@@ -682,7 +691,7 @@
         pltpu.VMEM((2, 16, 2048), BF16),
         pltpu.VMEM((32, 1152), BF16),
         sems((36,)), sems((36,)), sems((36,)), sems((8,)), sems((8,)), sems((8,)), sems((8,)),
-        sems((3,)), sems((9,)), sems((12,)), sems((7,)), sems((8,)), sems((11,)), sems((11,)), sems((10,)), sems((10,)),
+        sems((3,)), sems((9,)), sems((12,)), sems((7,)), sems((8,)), sems((11,)), sems((11,)), sems((20,)), sems((20,)),
         sems((16,)),
     ]
     return pl.pallas_call(

time: 88.4 us -> 88.6 us (level)
  no operation moved by 1% of the time
where the time goes in v4:
time: 88.6 us; the launch traced here: 88.5 us
  Pallas kernels  87.6 us (99%)
    pallas_call x1, Pallas kernels, shards(): pl.pallas_call(kernel, out_shape=jax.ShapeDtypeStruct((32, 2048), BF16),...  87.6 us

profile of v4, /device:TPU:1, one launch (start us, length us, event | category | flops | bytes accessed | tf_op | source)
XLA Modules:
  0.0 88.5 jit_solution(10413132902140478261)
XLA Ops:
  0.0 0.1 multiply_sine_fusion
  0.2 87.6 %shard_map.163 = bf16[32,2048]{1,0:T(8,128)(2,1)S(1)} custom-call(bf16[256,256]{1,0:T(8,128)(2,1)} %args_0_.4, f32[1,256]{1,0:T(1,128)} %bitcast.33, bf16[32,256]{1,0:T(8,128)(2,1)} %bitcast.30, f32[16,256]{1,0:T(8,128)S(1)} %get-tuple-element.6.args_3_, f32[16,256]{1,0:T(8,128)S(1)} %get-tuple-element.5.args_4_, bf16[160,256]{1,0:T(8,128)(2,1)} %bitcast.23, ...), custom_call_target="tpu_custom_call" | custom-call | tf_op jit(solution)/shard_map/pallas_call | solution.py:697
  87.8 0.7 copy.19
  (2 shorter events, 0.0 us)

commit v5 on v3

--- a/solution.py
+++ b/solution.py
@@ -481,7 +481,7 @@
     att[tp, 0:128, :] = (result[0:128] / total[:, 0:256]).astype(BF16)
     att[tp, 128:192, :] = (result[128:192] / total[:, 256:512]).astype(BF16)
 
-    weights.far(jnp.int32(11))
+    share_far()
 
     def att_copy(t, half, i, dev):
         ref = att.at[t] if half is None else att.at[t, half]
@@ -490,9 +490,7 @@
     for half, i, dev in ((top, 0, x_up), (low, 2, x_dn), (low, 1, x_up), (top, 3, x_dn), (None, 6, partner)):
         att_copy(tp, half, i, dev).start()
 
-    share_far()
-
-    @pl.loop(12, 15)
+    @pl.loop(11, 17)
     def _(n):
         weights.far(n)
 
@@ -501,13 +499,14 @@
     att_copy(t_up, top, 4, x_up).start()
     att_copy(t_dn, low, 2, partner).wait_recv()
     att_copy(t_dn, low, 5, x_dn).start()
-    weights.far(jnp.int32(15))
+    weights.far(jnp.int32(17))
+    weights.far(jnp.int32(18))
     att_copy(t_up, low, 1, partner).wait_recv()
     att_copy(t_up, None, 8, partner).start()
     att_copy(t_dn, top, 3, partner).wait_recv()
     att_copy(t_dn, None, 7, partner).start()
 
-    @pl.loop(16, 18)
+    @pl.loop(19, 21)
     def _(n):
         weights.far(n)
 
@@ -515,7 +514,8 @@
     att_copy(t_far, top, 9, partner).start()
     att_copy(t_far, low, 5, partner).wait_recv()
     att_copy(t_far, low, 10, partner).start()
-    weights.far(jnp.int32(18))
+    weights.far(jnp.int32(21))
+    weights.far(jnp.int32(22))
 
     for half, i in ((None, 6), (None, 7), (None, 8), (top, 9), (low, 10)):
         att_copy(tp, half, i, partner).wait_recv()
@@ -540,8 +540,8 @@
         for t in range(1, 8):
             acc = acc + jnp.dot(att_t[t], wout[t, :, cols], preferred_element_type=F32)
         hs[:, cols] = acc
-        weights.far(19 + 2 * j)
-        weights.far(20 + 2 * j)
+        weights.far(23 + 2 * j)
+        weights.far(24 + 2 * j)
 
     for i in range(7):
         remote(rows.at[tp], rows.at[tp], r_send.at[i], r_recv.at[tp], partner).wait_send()
@@ -556,9 +556,11 @@
         value = mixed.astype(F32)
         scale = lax.rsqrt(jnp.mean(value * value, axis=-1, keepdims=True) + EPS)
         norm[chunk, :] = (value * scale * mgain[...]).astype(BF16)
-        weights.far(27 + t)
-
-    weights.far(jnp.int32(35))
+
+        @pl.when(t < 5)
+        def _():
+            weights.far(31 + t)
+
 
     wts[sp] = wown[...]
     both = jnp.dot(norm[...], wts[:, :, 0:768].reshape(2048, 768), preferred_element_type=F32)

time: 88.4 us -> 87.8 us (level)
  no operation moved by 1% of the time
where the time goes in v5:
time: 87.8 us; the launch traced here: 87.6 us
  Pallas kernels  86.8 us (99%)
    pallas_call x1, Pallas kernels, shards(): pl.pallas_call(kernel, out_shape=jax.ShapeDtypeStruct((32, 2048), BF16),...  86.8 us

profile of v5, /device:TPU:1, one launch (start us, length us, event | category | flops | bytes accessed | tf_op | source)
XLA Modules:
  0.0 87.6 jit_solution(17554717618588579916)
XLA Ops:
  0.0 0.1 multiply_sine_fusion
  0.2 86.8 %shard_map.163 = bf16[32,2048]{1,0:T(8,128)(2,1)S(1)} custom-call(bf16[256,256]{1,0:T(8,128)(2,1)} %args_0_.4, f32[1,256]{1,0:T(1,128)} %bitcast.33, bf16[32,256]{1,0:T(8,128)(2,1)} %bitcast.30, f32[16,256]{1,0:T(8,128)S(1)} %get-tuple-element.6.args_3_, f32[16,256]{1,0:T(8,128)S(1)} %get-tuple-element.5.args_4_, bf16[160,256]{1,0:T(8,128)(2,1)} %bitcast.23, ...), custom_call_target="tpu_custom_call" | custom-call | tf_op jit(solution)/shard_map/pallas_call | solution.py:690
  87.0 0.7 copy.19
  (2 shorter events, 0.0 us)
